TPU v7x, 256 devices: a whole 4x4x8 slice. The times are simulated.
256 devices in a mesh: rep: 2 (over z_hi), fs: 16 (over z_lo, x), tp: 8 (over y, core).
Axes of the slice: x: 4, y: 4, z: 8 (z_hi: 2, z_lo: 4; z = z_hi * 4 + z_lo), core: 2. Of those that a mesh axis runs over, the one named last changes fastest.
Arguments:
- tokens: bfloat16 [32768, 2048], P(('rep', 'fs'), 'tp'), may hold values from -6 to 6
- mix_in_gain: bfloat16 [2048], replicated, may hold values from 0.099609375 to 1.8984375
- bgate_weight: bfloat16 [2048, 2048], P('fs', 'tp'), may hold values from -0.125 to 0.125
- cgate_weight: bfloat16 [2048, 2048], P('fs', 'tp'), may hold values from -0.125 to 0.125
- value_weight: bfloat16 [2048, 2048], P('fs', 'tp'), may hold values from -0.125 to 0.125
- conv_taps: bfloat16 [3, 2048], replicated, may hold values from -3 to 3
- out_weight: bfloat16 [2048, 2048], P('tp', 'fs'), may hold values from -0.41984465 to 0.41984465
- mix_out_gain: bfloat16 [2048], replicated, may hold values from 0.099609375 to 1.8984375
- ffn_in_gain: bfloat16 [2048], replicated, may hold values from 0.099609375 to 1.8984375
- up_weight: bfloat16 [2048, 8192], P('fs', 'tp'), may hold values from -0.125 to 0.125
- down_weight: bfloat16 [8192, 2048], P('tp', 'fs'), may hold values from -0.20992233 to 0.20992233
- ffn_out_gain: bfloat16 [2048], replicated, may hold values from 0.099609375 to 1.8984375
Outputs:
- result: bfloat16 [32768, 2048], P(('rep', 'fs'), 'tp')
All inputs are finite; a program needn't handle non-finite values.
Results may differ from a plain program's by a relative error of at most 0.02.
Values may be sent and summed in bfloat16 or wider, within the bound.
A program may use at most 128 MiB of HBM per device.

v0:
```python
import jax
import jax.numpy as jnp
from jax import lax
from jax.sharding import Mesh
from jax.sharding import PartitionSpec as P

LEN = 256
FS = ("fs_0", "fs_1")
REP_FS = ("rep", "fs_0", "fs_1")


epsilon = 1e-06


def in_order(pieces, dim):
    pieces = jnp.moveaxis(pieces, 0, dim)
    shape = pieces.shape
    return pieces.reshape(*shape[:dim], shape[dim] * shape[dim + 1], *shape[dim + 2 :])


def from_everyone(x, axis):
    length = lax.axis_size(axis)
    return lax.all_to_all(jnp.broadcast_to(x[None], (length, *x.shape)), axis, 0, 0, tiled=True)


def gathered_copies(x, axis, dim):
    return in_order(from_everyone(x, axis), dim)


def in_blocks(x, dim, length):
    before, after = (x.shape[:dim], x.shape[dim + 1 :])
    return jnp.moveaxis(x.reshape(*before, length, -1, *after), dim, 0)


def sent_and_summed(x, axis, dim):
    pieces = in_blocks(x, dim, lax.axis_size(axis))
    arrived = lax.all_to_all(pieces, axis, split_axis=0, concat_axis=0, tiled=True)
    return arrived.astype(jnp.float32).sum(axis=0)


def of_everyone(x, axis):
    everything = from_everyone(x, axis)
    return jnp.sum(everything, axis=0)


def all_blocks(x, axes, order):
    pieces = x
    for k in order:
        pieces = lax.all_gather(pieces, axes[k])
    done = order[::-1]
    back = [done.index(k) for k in range(len(axes))]
    pieces = pieces.transpose(*back, *range(len(axes), pieces.ndim))
    return pieces.reshape(-1, *x.shape)


def whole_of(x, axes, order, dim):
    return in_order(all_blocks(x, axes, order), dim)


def normalize(rows, gain):
    rows = rows.astype(jnp.float32)
    factor = lax.rsqrt(jnp.mean(rows * rows, axis=-1, keepdims=True) + epsilon)
    return rows * factor * gain.astype(jnp.float32)


def convolve(inner, taps):
    seqs = inner.reshape(-1, LEN, inner.shape[1])
    padded = jnp.pad(seqs, ((0, 0), (1, 1), (0, 0)))
    weights = taps.astype(jnp.float32)
    out = weights[0] * padded[:, :-2] + weights[1] * padded[:, 1:-1] + weights[2] * padded[:, 2:]
    return out.reshape(inner.shape)


def body(
    tokens,
    mix_in_gain,
    bgate_weight,
    cgate_weight,
    value_weight,
    conv_taps,
    out_weight,
    mix_out_gain,
    ffn_in_gain,
    up_weight,
    down_weight,
    ffn_out_gain,
):
    column = lax.axis_index("tp")
    own_width = tokens.shape[1]
    first = column * own_width
    full_width = mix_in_gain.shape[0]
    whole = lax.all_gather(tokens, "tp", axis=1, tiled=True)
    normed = normalize(whole, mix_in_gain).astype(jnp.bfloat16)

    def add_rows(piece):
        return jnp.dot(normed, piece, preferred_element_type=jnp.float32)

    bgate = add_rows(gathered_copies(bgate_weight, FS, 0))
    cgate = add_rows(gathered_copies(cgate_weight, FS, 0))
    value = add_rows(gathered_copies(value_weight, FS, 0))
    bgate = bgate.astype(jnp.bfloat16)
    cgate = cgate.astype(jnp.bfloat16)
    value = value.astype(jnp.bfloat16)
    channels = bgate.shape[1]
    own_taps = lax.dynamic_slice_in_dim(conv_taps, column * channels, channels, 1)
    inner = cgate.astype(jnp.float32) * value.astype(jnp.float32)
    gated = (bgate.astype(jnp.float32) * convolve(inner, own_taps)).astype(jnp.bfloat16)
    partial_mix = jnp.dot(
        gated, gathered_copies(out_weight, FS, 1), preferred_element_type=jnp.float32
    )
    mixed = sent_and_summed(partial_mix.astype(jnp.bfloat16), "tp", 1)
    power = of_everyone(jnp.sum(mixed * mixed, axis=1), "tp")
    gain_own = lax.dynamic_slice_in_dim(mix_out_gain, first, own_width, 0).astype(jnp.float32)
    scaled = mixed * lax.rsqrt(power[:, None] / full_width + epsilon) * gain_own
    resid_own = (tokens.astype(jnp.float32) + scaled).astype(jnp.bfloat16)
    resid = lax.all_gather(resid_own, "tp", axis=1, tiled=True)
    second = normalize(resid, ffn_in_gain).astype(jnp.bfloat16)
    lifted = jnp.dot(second, whole_of(up_weight, FS, (0, 1), 0), preferred_element_type=jnp.float32)
    active = jnp.square(jnp.maximum(lifted, 0.0)).astype(jnp.bfloat16)
    partial_ffn = jnp.dot(
        active, whole_of(down_weight, FS, (0, 1), 1), preferred_element_type=jnp.float32
    )
    ffn = sent_and_summed(partial_ffn.astype(jnp.bfloat16), "tp", 1)
    ffn_energy = of_everyone(jnp.sum(ffn * ffn, axis=1), "tp")
    out_gain = lax.dynamic_slice_in_dim(ffn_out_gain, first, own_width, 0).astype(jnp.float32)
    closing = ffn * lax.rsqrt(ffn_energy[:, None] / full_width + epsilon) * out_gain
    return (resid_own.astype(jnp.float32) + closing).astype(jnp.bfloat16)


def solution(mesh):
    torus = Mesh(
        mesh.devices.reshape(mesh.shape["rep"], 4, 4, mesh.shape["tp"]),
        ("rep", "fs_0", "fs_1", "tp"),
    )
    return jax.shard_map(
        body,
        mesh=torus,
        in_specs=(
            P(REP_FS, "tp"),
            P(),
            P(FS, "tp"),
            P(FS, "tp"),
            P(FS, "tp"),
            P(),
            P("tp", FS),
            P(),
            P(),
            P(FS, "tp"),
            P("tp", FS),
            P(),
        ),
        out_specs=P(REP_FS, "tp"),
        check_vma=False,
    )
```

profile of v0, /device:TPU:1, one launch (start us, length us, event | category | flops | bytes accessed | tf_op | source)
XLA Modules:
  0.0 391.8 jit_solution(6726258593251835402)
XLA Ops:
  8.8 36.9 %all-gather.19.cloned.1.call-done = bf16[4096,128]{1,0:T(8,128)(2,1)} async-done(((bf16[1024,128]{1,0:T(8,128)(2,1)}), bf16[4096,128]{1,0:T(8,128)(2,1)}) %all-gather.19.cloned.1.call-update) | async-done | bytes 1048592 | tf_op jit(solution)/shard_map/all_gather | solution.py:49
  45.8 0.9 broadcast_in_dim.13
  46.7 40.9 %all_to_all.42 = bf16[16,128,256]{2,1,0:T(8,128)(2,1)S(1)} all-to-all(bf16[16,128,256]{2,1,0:T(8,128)(2,1)S(1)} %broadcast_in_dim.13), channel_id=1, replica_groups=mesh['rep'=2,'fs_0'=4,'fs_1'=4,'tp'=8] {'fs_0','fs_1'}, dimensions={0} | all-to-all | bytes 2097152 | tf_op jit(solution)/shard_map/all_to_all | solution.py:23
  87.6 1.1 broadcast_in_dim.14
  88.7 9.8 %all-to-all-start.2 = ((bf16[16,128,256]{2,1,0:T(8,128)(2,1)}), bf16[16,128,256]{2,1,0:T(8,128)(2,1)S(1)}, u32[]{:S(2)}, u32[]{:S(2)}) async-start(bf16[16,128,256]{2,1,0:T(8,128)(2,1)} %broadcast_in_dim.14), calls=%async_computation.2 | async-start | bytes 2097152 | tf_op jit(solution)/shard_map/all_to_all | solution.py:23
  98.6 21.9 %all-to-all-done.2 = bf16[16,128,256]{2,1,0:T(8,128)(2,1)S(1)} async-done(((bf16[16,128,256]{2,1,0:T(8,128)(2,1)}), bf16[16,128,256]{2,1,0:T(8,128)(2,1)S(1)}, u32[]{:S(2)}, u32[]{:S(2)}) %all-to-all-start.2) | async-done | bytes 1048608 | tf_op jit(solution)/shard_map/all_to_all | solution.py:23
  120.5 1.1 broadcast_in_dim.15
  121.5 7.9 %all-to-all-start.3 = ((bf16[16,256,128]{1,2,0:T(8,128)(2,1)}), bf16[16,256,128]{1,2,0:T(8,128)(2,1)S(1)}, u32[]{:S(2)}, u32[]{:S(2)}) async-start(bf16[16,256,128]{1,2,0:T(8,128)(2,1)} %broadcast_in_dim.15), calls=%async_computation.3 | async-start | bytes 2097152 | tf_op jit(solution)/shard_map/all_to_all | solution.py:23
  130.1 21.5 %all-to-all-done.3 = bf16[16,256,128]{1,2,0:T(8,128)(2,1)S(1)} async-done(((bf16[16,256,128]{1,2,0:T(8,128)(2,1)}), bf16[16,256,128]{1,2,0:T(8,128)(2,1)S(1)}, u32[]{:S(2)}, u32[]{:S(2)}) %all-to-all-start.3) | async-done | bytes 1048608 | tf_op jit(solution)/shard_map/all_to_all | solution.py:23
  151.6 1.2 broadcast_in_dim.12
  152.8 7.8 %all-to-all-start = ((bf16[16,128,256]{2,1,0:T(8,128)(2,1)}), bf16[16,128,256]{2,1,0:T(8,128)(2,1)}, u32[]{:S(2)}, u32[]{:S(2)}) async-start(bf16[16,128,256]{2,1,0:T(8,128)(2,1)} %broadcast_in_dim.12), calls=%async_computation | async-start | bytes 2097152 | tf_op jit(solution)/shard_map/all_to_all | solution.py:23
  161.2 3.2 fusion
  164.7 1.3 fusion.13
  166.0 1.3 fusion.12
  167.7 15.1 %all-to-all-done = bf16[16,128,256]{2,1,0:T(8,128)(2,1)} async-done(((bf16[16,128,256]{2,1,0:T(8,128)(2,1)}), bf16[16,128,256]{2,1,0:T(8,128)(2,1)}, u32[]{:S(2)}, u32[]{:S(2)}) %all-to-all-start) | async-done | bytes 1048608 | tf_op jit(solution)/shard_map/all_to_all | solution.py:23
  182.8 8.8 %convolution_convert_fusion = bf16[1024,2048]{1,0:T(8,128)(2,1)} fusion(bf16[256,2048]{0,1:T(8,128)(2,1)S(1)} %bitcast.55, f32[1024,256]{1,0:T(8,128)S(1)} %bitcast.58, bf16[2048,256]{1,0:T(8,128)(2,1)} %bitcast, bf16[1024,2048]{1,0:T(8,128)(2,1)} %all-gather.11.cloned.1.call-done, f32[2048]{0:T(1024)S(1)} %convert_element_type.79, ...), kind=kOutput, calls=%fused_computation.18 | convolution fusion | flops 2159017984 | bytes 11546624 | tf_op jit(solution)/shard_map/dot_general | solution.py:108
  191.7 2.5 copy.46
  194.1 56.0 %all_to_all.43 = bf16[8,1024,256]{2,1,0:T(8,128)(2,1)S(1)} all-to-all(bf16[8,1024,256]{2,1,0:T(8,128)(2,1)S(1)} %bitcast.44), channel_id=1, replica_groups=mesh['rep'=2,'fs_0'=4,'fs_1'=4,'tp'=8] {'tp'}, dimensions={0} | all-to-all | bytes 8388608 | tf_op jit(solution)/shard_map/all_to_all | solution.py:37
  251.6 4.2 %all-to-all-start.5 = ((f32[8,1,1024]{2,1,0:T(1,128)}), f32[8,1,1024]{2,1,0:T(1,128)S(1)}, u32[]{:S(2)}, u32[]{:S(2)}) async-start(f32[8,1,1024]{2,1,0:T(1,128)} %broadcast_in_dim.16), calls=%async_computation.5 | async-start | bytes 65536 | tf_op jit(solution)/shard_map/all_to_all | solution.py:23
  256.6 4.0 %all-to-all-done.5 = f32[8,1,1024]{2,1,0:T(1,128)S(1)} async-done(((f32[8,1,1024]{2,1,0:T(1,128)}), f32[8,1,1024]{2,1,0:T(1,128)S(1)}, u32[]{:S(2)}, u32[]{:S(2)}) %all-to-all-start.5) | async-done | bytes 32800 | tf_op jit(solution)/shard_map/all_to_all | solution.py:23
  260.6 1.1 add_convert_fusion.1
  261.8 4.5 %copy.35 = bf16[4,4,1024,128]{3,2,1,0:T(8,128)(2,1)} copy(bf16[4,4,1024,128]{3,2,0,1:T(8,128)(2,1)} %bitcast.47) | data formatting | bytes 8388608 | tf_op jit(solution)/shard_map/transpose | solution.py:52
  266.3 6.4 %copy.36 = bf16[1024,16,128]{0,2,1:T(8,128)(2,1)} copy(bf16[1024,16,128]{2,0,1:T(8,128)(2,1)} %bitcast.45) | data formatting | bytes 8388608 | tf_op jit(solution)/shard_map/transpose | solution.py:16
  272.7 5.0 %copy.34 = bf16[4,4,128,1024]{3,2,1,0:T(8,128)(2,1)} copy(bf16[4,4,128,1024]{3,2,0,1:T(8,128)(2,1)} %bitcast.48) | data formatting | bytes 8388608 | tf_op jit(solution)/shard_map/transpose | solution.py:52
  277.7 22.9 %all-gather.13.cloned.1.call-done = bf16[1024,2048]{1,0:T(8,128)(2,1)} async-done(((bf16[1024,256]{1,0:T(8,128)(2,1)}), bf16[1024,2048]{1,0:T(8,128)(2,1)}) %all-gather.13.cloned.1.call-update) | async-done | bytes 4194320 | tf_op jit(solution)/shard_map/all_gather | solution.py:116
  300.6 3.1 fusion.3
  303.7 14.6 %convolution_convert_fusion.1 = bf16[1024,2048]{1,0:T(8,128)(2,1)} fusion(bf16[1024,2048]{0,1:T(8,128)(2,1)} %bitcast.49, bf16[2048,1024]{1,0:T(8,128)(2,1)} %bitcast.50, bf16[1024,2048]{1,0:T(8,128)(2,1)} %all-gather.13.cloned.1.call-done, f32[2048]{0:T(1024)S(1)} %convert_element_type.95, f32[1024]{0:T(1024)S(1)} %add_rsqrt_fusion.1), kind=kOutput, calls=%fused_computation.19 | convolution fusion | flops 8603566080 | bytes 16789504 | tf_op jit(solution)/shard_map/dot_general | solution.py:120
  318.3 2.5 copy.45
  320.8 52.6 %all_to_all.44 = bf16[8,1024,256]{2,1,0:T(8,128)(2,1)S(1)} all-to-all(bf16[8,1024,256]{2,1,0:T(8,128)(2,1)S(1)} %bitcast.46), channel_id=1, replica_groups=mesh['rep'=2,'fs_0'=4,'fs_1'=4,'tp'=8] {'tp'}, dimensions={0} | all-to-all | bytes 8388608 | tf_op jit(solution)/shard_map/all_to_all | solution.py:37
  374.8 4.3 %all-to-all-start.7 = ((f32[8,1,1024]{2,1,0:T(1,128)}), f32[8,1,1024]{2,1,0:T(1,128)S(1)}, u32[]{:S(2)}, u32[]{:S(2)}) async-start(f32[8,1,1024]{2,1,0:T(1,128)} %broadcast_in_dim.17), calls=%async_computation.7 | async-start | bytes 65536 | tf_op jit(solution)/shard_map/all_to_all | solution.py:23
  379.9 4.0 %all-to-all-done.7 = f32[8,1,1024]{2,1,0:T(1,128)S(1)} async-done(((f32[8,1,1024]{2,1,0:T(1,128)}), f32[8,1,1024]{2,1,0:T(1,128)S(1)}, u32[]{:S(2)}, u32[]{:S(2)}) %all-to-all-start.7) | async-done | bytes 32800 | tf_op jit(solution)/shard_map/all_to_all | solution.py:23
  383.9 1.1 add_convert_fusion
  (52 shorter events, 8.7 us)
Async XLA Ops:
  6.5 81.1 %copy-start.3 = (bf16[128,256]{1,0:T(8,128)(2,1)S(1)}, bf16[128,256]{1,0:T(8,128)(2,1)}, u32[]{:S(2)}) copy-start(bf16[128,256]{1,0:T(8,128)(2,1)} %param.16) | copy-start | bytes 196612
  6.5 39.2 %all-gather.19.cloned.1.call-start = ((), (), s32[]{:S(2)}) async-start(), calls=%async_computation.12 | async-start | bytes 1310720 | tf_op jit(solution)/shard_map/all_gather | solution.py:49
  7.3 91.2 %copy-start.5 = (bf16[256,128]{1,0:T(8,128)(2,1)S(1)}, bf16[256,128]{1,0:T(8,128)(2,1)}, u32[]{:S(2)}) copy-start(bf16[256,128]{1,0:T(8,128)(2,1)} %param.18) | copy-start | bytes 196612
  7.3 153.4 %all-gather.15.cloned.1.call-start = ((), (), s32[]{:S(2)}) async-start(), calls=%async_computation.10 | async-start | bytes 1310720 | tf_op jit(solution)/shard_map/all_gather | solution.py:49
  8.0 153.2 %all-gather.11.cloned.1.call-start = ((), (), s32[]{:S(2)}) async-start(), calls=%async_computation.8 | async-start | bytes 4718592 | tf_op jit(solution)/shard_map/all_gather | solution.py:92
  8.8 253.0 %all-gather.21.cloned.1.call-start = ((), (), s32[]{:S(2)}) async-start(), calls=%async_computation.13 | async-start | bytes 5242880 | tf_op jit(solution)/shard_map/all_gather | solution.py:49
  46.7 104.9 %copy-start.4 = (bf16[128,256]{1,0:T(8,128)(2,1)S(1)}, bf16[128,256]{1,0:T(8,128)(2,1)}, u32[]{:S(2)}) copy-start(bf16[128,256]{1,0:T(8,128)(2,1)} %param.14) | copy-start | bytes 196612
  88.7 72.0 %copy-start.6 = (bf16[2048]{0:T(1024)(128)(2,1)S(1)}, bf16[2048]{0:T(1024)(128)(2,1)}, u32[]{:S(2)}) copy-start(bf16[2048]{0:T(1024)(128)(2,1)} %param.13) | copy-start | bytes 12292
  88.7 31.8 %all-to-all-start.2 = ((bf16[16,128,256]{2,1,0:T(8,128)(2,1)}), bf16[16,128,256]{2,1,0:T(8,128)(2,1)S(1)}, u32[]{:S(2)}, u32[]{:S(2)}) async-start(bf16[16,128,256]{2,1,0:T(8,128)(2,1)} %broadcast_in_dim.14), calls=%async_computation.2 | async-start | bytes 2097152 | tf_op jit(solution)/shard_map/all_to_all | solution.py:23
  121.5 30.1 %all-to-all-start.3 = ((bf16[16,256,128]{1,2,0:T(8,128)(2,1)}), bf16[16,256,128]{1,2,0:T(8,128)(2,1)S(1)}, u32[]{:S(2)}, u32[]{:S(2)}) async-start(bf16[16,256,128]{1,2,0:T(8,128)(2,1)} %broadcast_in_dim.15), calls=%async_computation.3 | async-start | bytes 2097152 | tf_op jit(solution)/shard_map/all_to_all | solution.py:23
  152.8 30.1 %all-to-all-start = ((bf16[16,128,256]{2,1,0:T(8,128)(2,1)}), bf16[16,128,256]{2,1,0:T(8,128)(2,1)}, u32[]{:S(2)}, u32[]{:S(2)}) async-start(bf16[16,128,256]{2,1,0:T(8,128)(2,1)} %broadcast_in_dim.12), calls=%async_computation | async-start | bytes 2097152 | tf_op jit(solution)/shard_map/all_to_all | solution.py:23
  160.6 112.1 %all-gather.17.cloned.1.call-start = ((), (), s32[]{:S(2)}) async-start(), calls=%async_computation.11 | async-start | bytes 5242880 | tf_op jit(solution)/shard_map/all_gather | solution.py:49
  161.2 3.5 copy-start.1
  250.2 10.5 %copy-start.2 = (bf16[1024,256]{1,0:T(8,128)(2,1)S(1)}, bf16[1024,256]{1,0:T(8,128)(2,1)}, u32[]{:S(2)}) copy-start(bf16[1024,256]{1,0:T(8,128)(2,1)} %param.12) | copy-start | bytes 1572868
  250.2 11.5 %copy-start.7 = (bf16[2048]{0:T(1024)(128)(2,1)S(1)}, bf16[2048]{0:T(1024)(128)(2,1)}, u32[]{:S(2)}) copy-start(bf16[2048]{0:T(1024)(128)(2,1)} %param.20) | copy-start | bytes 12292
  251.6 9.0 %all-to-all-start.5 = ((f32[8,1,1024]{2,1,0:T(1,128)}), f32[8,1,1024]{2,1,0:T(1,128)S(1)}, u32[]{:S(2)}, u32[]{:S(2)}) async-start(f32[8,1,1024]{2,1,0:T(1,128)} %broadcast_in_dim.16), calls=%async_computation.5 | async-start | bytes 65536 | tf_op jit(solution)/shard_map/all_to_all | solution.py:23
  255.8 44.7 %all-gather.13.cloned.1.call-start = ((), (), s32[]{:S(2)}) async-start(), calls=%async_computation.9 | async-start | bytes 4718592 | tf_op jit(solution)/shard_map/all_gather | solution.py:116
  373.4 10.5 %copy-start = (bf16[1024,256]{1,0:T(8,128)(2,1)S(1)}, bf16[1024,256]{1,0:T(8,128)(2,1)}, u32[]{:S(2)}) copy-start(bf16[1024,256]{1,0:T(8,128)(2,1)} %add_convert_fusion.1) | copy-start | bytes 1572868
  374.8 9.0 %all-to-all-start.7 = ((f32[8,1,1024]{2,1,0:T(1,128)}), f32[8,1,1024]{2,1,0:T(1,128)S(1)}, u32[]{:S(2)}, u32[]{:S(2)}) async-start(f32[8,1,1024]{2,1,0:T(1,128)} %broadcast_in_dim.17), calls=%async_computation.7 | async-start | bytes 65536 | tf_op jit(solution)/shard_map/all_to_all | solution.py:23
Sparse Core Ops, SparseCore 0:
  9.1 36.5 all-gather.18
  47.5 43.0 all-gather.14
  92.5 42.0 all-gather.10
  136.3 62.9 all-gather.20
  200.9 51.1 all-gather.16
  261.8 38.7 all-gather.12
where the time goes:
time: 393 us; the launch traced here: 392 us
  blocking collectives  150 us (38%)
  waiting for transfers between devices  129 us (33%)
  starting transfers between devices  34.2 us (9%)
  local copies, waits for them, and re-layouts  26.7 us (7%)
  matrix products  26.1 us (7%)
  between operations  13.7 us (3%)
  other arithmetic  12.6 us (3%)
    all_to_all x2, blocking collectives, sent_and_summed(): lax.all_to_all(pieces, axis, split_axis=0, concat_axis=0, tiled=True)  109 us
    all_to_all x5, waiting for transfers between devices, from_everyone(): lax.all_to_all(jnp.broadcast_to(x[None], (length, *x.shape)), axis, 0, 0,...  66.5 us
    all_to_all x1, blocking collectives, from_everyone(): lax.all_to_all(jnp.broadcast_to(x[None], (length, *x.shape)), axis, 0, 0,...  40.9 us
    all_gather x4, waiting for transfers between devices, all_blocks(): pieces = lax.all_gather(pieces, axes[k])  37 us
    all_to_all x5, starting transfers between devices, from_everyone(): lax.all_to_all(jnp.broadcast_to(x[None], (length, *x.shape)), axis, 0, 0,...  34 us
    all_gather x1, waiting for transfers between devices, body(): resid = lax.all_gather(resid_own, 'tp', axis=1, tiled=True)  22.9 us
    dot_general x1, matrix products, body(): jnp.dot(active, whole_of(down_weight, FS, (0, 1), 1), preferred_element_t...  14.6 us
    transpose x2, local copies, waits for them, and re-layouts, all_blocks(): pieces = pieces.transpose(*back, *range(len(axes), pieces.ndim))  9.5 us
  transfers between devices with their start and end apart: 11, of which 7 were waited for; matrix products, arithmetic and copies ran while one was open for 11% of the time, Pallas kernels for 0%

commit v1 on v0

v1 whole, which is shorter than its diff:
```python
import jax
import jax.numpy as jnp
from jax import lax
from jax.experimental import pallas as pl
from jax.experimental.pallas import tpu as pltpu
from jax.sharding import Mesh
from jax.sharding import PartitionSpec as P

EPS = 1e-6
F32 = jnp.float32
BF16 = jnp.bfloat16
LEN = 256
ROWS = 1024
W = 256
NSEQ = ROWS // LEN
NSEM = 256


class Link:
    def __init__(self, send, recv, first):
        self.send, self.recv, self.used, self.open = send, recv, first, []

    def start(self, src, dst, landed, device):
        k = self.used
        self.used += 1
        copy = pltpu.make_async_remote_copy(
            src_ref=src, dst_ref=dst, send_sem=self.send.at[k], recv_sem=self.recv.at[k],
            device_id=device, device_id_type=pl.DeviceIdType.MESH,
        )
        copy.start()
        arrival = pltpu.make_async_remote_copy(
            src_ref=landed, dst_ref=landed, send_sem=self.send.at[k], recv_sem=self.recv.at[k],
            device_id=device, device_id_type=pl.DeviceIdType.MESH,
        )
        self.open.append(copy)
        return arrival.wait_recv

    def same(self, mine, theirs, device):
        return self.start(mine, mine, theirs, device)

    def drain(self):
        for copy in self.open:
            copy.wait_send()
        self.open = []


class Here:
    def __init__(self):
        r, z, x, y, c = (lax.axis_index(n) for n in ("r", "z", "x", "y", "c"))
        self.z, self.x, self.y, self.c = z, x, y, c
        plus = lambda v, k, n: lax.rem(v + k, n)
        self.xp, self.xo, self.xm = (plus(x, k, 4) for k in (1, 2, 3))
        self.yp, self.yo, self.ym = (plus(y, k, 4) for k in (1, 2, 3))
        self.zp, self.zo, self.zm = (plus(z, k, 4) for k in (1, 2, 3))
        self.cn = 1 - c
        up, down = plus(r * 4 + z, 1, 8), plus(r * 4 + z, 7, 8)
        self.to_xp, self.to_xm = {"x": self.xp}, {"x": self.xm}
        self.to_yp, self.to_ym = {"y": self.yp}, {"y": self.ym}
        self.to_zp = {"r": up // 4, "z": lax.rem(up, 4)}
        self.to_zm = {"r": down // 4, "z": lax.rem(down, 4)}
        self.to_mate = {"c": self.cn}
        self.col = y * 2 + c


def at128(v, n=128):
    return pl.ds(pl.multiple_of(v * 128, 128), n)


class Weight:
    def __init__(self, link, here, buf, by_row):
        self.link, self.h, self.buf, self.by_row = link, here, buf, by_row
        self.half = (buf.shape[2] if by_row else buf.shape[1]) // 2

    def unit(self, z, x, part, half=None):
        if self.by_row:
            start, n = (0, 128) if half is None else (64 * half, 64)
            rows = pl.ds(pl.multiple_of(x * 128 + start, 64), n)
            return self.buf.at[z, rows, pl.ds(part * self.half, self.half)]
        q = self.half // 2
        rows = pl.ds(part * self.half, self.half) if half is None else pl.ds(part * self.half + half * q, q)
        return self.buf.at[z, rows, at128(x)]

    def line_a(self, z, half):
        if self.by_row:
            return self.buf.at[z, pl.ds(256 * half, 256), pl.ds(0, self.half)]
        q = self.half // 2
        return self.buf.at[z, pl.ds(q * half, q), :]

    def line_b(self, x, half):
        if self.by_row:
            return self.buf.at[pl.ds(2 * half, 2), at128(x), pl.ds(self.half, self.half)]
        return self.buf.at[pl.ds(2 * half, 2), pl.ds(self.half, self.half), at128(x)]

    def p1(self):
        h, u, s = self.h, self.unit, self.link.same
        a, b = u(h.z, h.x, 0), u(h.z, h.x, 1)
        self.r1 = [
            s(a, u(h.z, h.xm, 0), h.to_xp), s(a, u(h.z, h.xp, 0), h.to_xm),
            s(b, u(h.zm, h.x, 1), h.to_zp), s(b, u(h.zp, h.x, 1), h.to_zm),
        ]

    def s1(self):
        h, u, s = self.h, self.unit, self.link.same
        self.r2 = []
        for k, (wait, src, gets, dev) in enumerate((
            (self.r1[0], u(h.z, h.xm, 0, 0), u(h.z, h.xo, 0, 0), h.to_xp),
            (self.r1[1], u(h.z, h.xp, 0, 1), u(h.z, h.xo, 0, 1), h.to_xm),
            (self.r1[2], u(h.zm, h.x, 1, 0), u(h.zo, h.x, 1, 0), h.to_zp),
            (self.r1[3], u(h.zp, h.x, 1, 1), u(h.zo, h.x, 1, 1), h.to_zm),
        )):
            wait()
            self.r2.append(s(src, gets, dev))

    def s2(self):
        h, s, a, b = self.h, self.link.same, self.line_a, self.line_b
        for wait in self.r2:
            wait()
        self.rf = [
            s(a(h.z, 0), a(h.zm, 0), h.to_zp), s(a(h.z, 1), a(h.zp, 1), h.to_zm),
            s(b(h.x, 0), b(h.xm, 0), h.to_xp), s(b(h.x, 1), b(h.xp, 1), h.to_xm),
        ]
        self.rg = [
            s(a(h.z, 1), a(h.zm, 1), h.to_zp), s(a(h.z, 0), a(h.zp, 0), h.to_zm),
            s(b(h.x, 1), b(h.xm, 1), h.to_xp), s(b(h.x, 0), b(h.xp, 0), h.to_xm),
        ]

    def s3(self):
        h, s, a, b = self.h, self.link.same, self.line_a, self.line_b
        for wait, src, gets, dev in (
            (self.rf[0], a(h.zm, 0), a(h.zo, 0), h.to_zp),
            (self.rf[1], a(h.zp, 1), a(h.zo, 1), h.to_zm),
            (self.rf[2], b(h.xm, 0), b(h.xo, 0), h.to_xp),
            (self.rf[3], b(h.xp, 1), b(h.xo, 1), h.to_xm),
        ):
            wait()
            self.rg.append(s(src, gets, dev))

    def s4(self):
        for wait in self.rg:
            wait()


class Gather:
    def __init__(self, link, here, buf, row, n):
        self.link, self.h, self.buf, self.row, self.n = link, here, buf, row, n

    def piece(self, c, y, half=None):
        if half is None:
            return self.buf.at[c, y, pl.ds(self.row, self.n)]
        return self.buf.at[c, y, pl.ds(self.row + half * (self.n // 2), self.n // 2)]

    def t0(self):
        h, s, p = self.h, self.link.same, self.piece
        c, y = h.c, h.y
        self.f = [s(p(c, y, 0), p(c, h.ym, 0), h.to_yp), s(p(c, y, 1), p(c, h.yp, 1), h.to_ym)]
        self.g = [s(p(c, y, 1), p(c, h.ym, 1), h.to_yp), s(p(c, y, 0), p(c, h.yp, 0), h.to_ym)]
        self.mate = [s(p(c, y), p(h.cn, y), h.to_mate)]

    def t1(self):
        h, s, p = self.h, self.link.same, self.piece
        c = h.c
        self.f[0]()
        far = [s(p(c, h.ym, 0), p(c, h.yo, 0), h.to_yp)]
        self.f[1]()
        far.append(s(p(c, h.yp, 1), p(c, h.yo, 1), h.to_ym))
        self.far = far
        self.g[0]()
        self.mate.append(s(p(c, h.ym), p(h.cn, h.ym), h.to_mate))
        self.g[1]()
        self.mate.append(s(p(c, h.yp), p(h.cn, h.yp), h.to_mate))

    def t2(self):
        h, s, p = self.h, self.link.same, self.piece
        for wait in self.far:
            wait()
        self.mate.append(s(p(h.c, h.yo), p(h.cn, h.yo), h.to_mate))

    def t3(self):
        for wait in self.mate:
            wait()


class Reduce:
    def __init__(self, link, here, part, mate, r1, r2, seq):
        self.link, self.h, self.part, self.mate, self.r1, self.r2 = link, here, part, mate, r1, r2
        self.seq, self.row = seq, seq * LEN

    def start(self):
        h, rows = self.h, pl.ds(self.row, LEN)
        self.w0 = self.link.start(
            self.part.at[h.cn, :, rows], self.mate.at[:, rows], self.mate.at[:, rows], h.to_mate
        )

    def both(self, y, lo=0, n=LEN):
        rows = pl.ds(self.row + lo, n)
        return self.part[self.h.c, y, rows, :].astype(F32) + self.mate[y, rows, :].astype(F32)

    def b(self):
        h, half = self.h, LEN // 2
        self.w0()
        self.part[h.c, h.yo, pl.ds(self.row, LEN), :] = self.both(h.yo).astype(BF16)
        lo = self.part.at[h.c, h.yo, pl.ds(self.row, half)]
        hi = self.part.at[h.c, h.yo, pl.ds(self.row + half, half)]
        d0, d1 = self.r1.at[0, self.seq], self.r1.at[1, self.seq]
        self.w1 = [self.link.start(lo, d0, d0, h.to_yp), self.link.start(hi, d1, d1, h.to_ym)]

    def c(self):
        h, half = self.h, LEN // 2
        rows = pl.ds(self.row, LEN)
        self.w2 = []
        for k, y, dev in ((0, h.yp, h.to_yp), (1, h.ym, h.to_ym)):
            self.w1[k]()
            add = self.r1[k, self.seq].astype(F32)
            near, far = self.both(y, k * half, half) + add, self.both(y, (1 - k) * half, half)
            self.part[h.c, y, pl.ds(self.row + k * half, half), :] = near.astype(BF16)
            self.part[h.c, y, pl.ds(self.row + (1 - k) * half, half), :] = far.astype(BF16)
            dst = self.r2.at[k, rows]
            self.w2.append(self.link.start(self.part.at[h.c, y, rows], dst, dst, dev))

    def d(self):
        rows = pl.ds(self.row, LEN)
        self.w2[0]()
        self.w2[1]()
        return self.both(self.h.y) + self.r2[0, rows, :].astype(F32) + self.r2[1, rows, :].astype(F32)


def mean_factor(total):
    return lax.rsqrt(total * (1.0 / (8 * W)) + EPS)


def kernel(
    tok, bw, cw, vw, ow, uw, dw, consts, out,
    X, M, N, WB, WO, WU, WD, ACT, PA, RDA, R1A, R2A, PB, RDB, R1B, R2B, OWN, ST,
    send, recv, local,
):
    h = Here()
    link, early = Link(send, recv, 32), Link(send, recv, 0)
    own_rows = at128(h.x)
    loads = [
        pltpu.make_async_copy(tok, X.at[h.c, h.y], local.at[0]),
        pltpu.make_async_copy(bw, WB.at[h.z, own_rows, pl.ds(0, W)], local.at[1]),
        pltpu.make_async_copy(cw, WB.at[h.z, own_rows, pl.ds(W, W)], local.at[2]),
        pltpu.make_async_copy(vw, WB.at[h.z, own_rows, pl.ds(2 * W, W)], local.at[3]),
        pltpu.make_async_copy(ow, WO.at[h.z, :, own_rows], local.at[4]),
        pltpu.make_async_copy(uw, WU.at[h.z, own_rows, :], local.at[5]),
        pltpu.make_async_copy(dw, WD.at[h.z, :, own_rows], local.at[6]),
    ]
    for load in loads:
        load.start()

    peers = [
        (dy, dc, {"y": lax.rem(h.y + dy, 4), "c": lax.rem(h.c + dc, 2)})
        for dy in range(4) for dc in range(2) if dy or dc
    ]
    barrier = pltpu.get_barrier_semaphore()
    targets = [h.to_xp, h.to_xm, h.to_zp, h.to_zm] + [dev for _, _, dev in peers]
    for dev in targets:
        pl.semaphore_signal(barrier, inc=1, device_id=dev, device_id_type=pl.DeviceIdType.MESH)
    pl.semaphore_wait(barrier, len(targets))

    toks = [Gather(early, h, X, t * 512, 512) for t in range(2)]
    bcv, outw = Weight(link, h, WB, True), Weight(link, h, WO, False)
    up, down = Weight(link, h, WU, True), Weight(link, h, WD, False)
    mix = [Reduce(link, h, PA, RDA, R1A, R2A, s) for s in range(NSEQ)]
    ffn = [Reduce(link, h, PB, RDB, R1B, R2B, s) for s in range(NSEQ)]
    mids = [Gather(link, h, M, s * LEN, LEN) for s in range(NSEQ)]

    def whole(buf, rows):
        return [buf[j % 2, j // 2, rows, :].astype(F32) for j in range(8)]

    def total(pieces):
        squares = sum(p * p for p in pieces)
        return jnp.sum(squares, axis=1, keepdims=True)

    def gain(k, j):
        return consts[k : k + 1, j * W : (j + 1) * W]

    def norm_tokens(first, count):
        def tile(i, carry):
            rows = pl.ds(pl.multiple_of(first + i * 16, 16), 16)
            pieces = whole(X, rows)
            factor = mean_factor(total(pieces))
            for j in range(8):
                N[rows, j * W : (j + 1) * W] = (pieces[j] * factor * gain(0, j)).astype(BF16)
            return carry

        lax.fori_loop(0, count // 16, tile, 0)

    position = lax.broadcasted_iota(jnp.int32, (LEN, W), 0)
    own_cols = pl.ds(pl.multiple_of(h.col * W, W), W)

    def mixer(s):
        rows = pl.ds(s * LEN, LEN)
        three = jnp.dot(N[rows, :], WB[...].reshape(8 * W, 3 * W), preferred_element_type=F32)
        b, c, v = (three[:, k * W : (k + 1) * W].astype(BF16).astype(F32) for k in range(3))
        inner = c * v
        before = jnp.where(position == 0, 0.0, pltpu.roll(inner, 1, 0))
        after = jnp.where(position == LEN - 1, 0.0, pltpu.roll(inner, LEN - 1, 0))
        taps = [consts[4 + k : 5 + k, own_cols] for k in range(3)]
        conv = taps[0] * before + taps[1] * inner + taps[2] * after
        return (b * conv).astype(BF16)

    def spread(left, weight, part, s):
        rows = pl.ds(s * LEN, LEN)
        for y in range(4):
            piece = jnp.dot(left, weight[y], preferred_element_type=F32).astype(BF16)
            part[0, y, rows, :] = piece[:, :W]
            part[1, y, rows, :] = piece[:, W:]

    def A(s, before_out=None):
        gated = mixer(s)
        if before_out:
            before_out()
        spread(gated, WO, PA, s)
        mix[s].start()

    def B(s):
        mix[s].b()

    def C(s):
        mix[s].c()

    def D(s):
        M[h.c, h.y, pl.ds(s * LEN, LEN), :] = mix[s].d().astype(BF16)
        mids[s].t0()

    def E(s):
        mids[s].t1()

    def F(s):
        mids[s].t2()

    def G(s):
        mids[s].t3()

        def tile(i, carry):
            rows = pl.ds(pl.multiple_of(s * LEN + i * 16, 16), 16)
            mixed = whole(M, rows)
            factor = mean_factor(total(mixed))
            pieces = []
            for j in range(8):
                r = X[j % 2, j // 2, rows, :].astype(F32) + mixed[j] * factor * gain(1, j)
                r = r.astype(BF16)
                X[j % 2, j // 2, rows, :] = r
                pieces.append(r.astype(F32))
            factor = mean_factor(total(pieces))
            for j in range(8):
                N[rows, j * W : (j + 1) * W] = (pieces[j] * factor * gain(2, j)).astype(BF16)
            return carry

        lax.fori_loop(0, LEN // 16, tile, 0)
        rows = pl.ds(s * LEN, LEN)
        lifted = jnp.dot(N[rows, :], WU[...].reshape(8 * W, 4 * W), preferred_element_type=F32)
        lifted = jnp.maximum(lifted, 0.0)
        ACT[rows, :] = (lifted * lifted).astype(BF16)

    def H(s):
        spread(ACT[pl.ds(s * LEN, LEN), :], WD, PB, s)
        ffn[s].start()

    def D2(s):
        own = ffn[s].d()
        OWN[pl.ds(s * LEN, LEN), :] = own
        ST[h.col, s : s + 1, :] = jnp.sum((own * own).T, axis=0, keepdims=True)

    loads[0].wait()
    toks[0].t0()
    toks[1].t0()
    for load in loads[1:4]:
        load.wait()
    bcv.p1()
    loads[4].wait()
    outw.p1()
    loads[5].wait()
    up.p1()
    loads[6].wait()
    ST[h.col] = jnp.zeros((8, W), F32)

    bcv.s1()
    outw.s1()
    bcv.s2()
    toks[0].t1()
    outw.s2()
    toks[1].t1()
    bcv.s3()
    up.s1()
    toks[0].t2()
    outw.s3()
    toks[0].t3()
    norm_tokens(0, 512)
    toks[1].t2()
    toks[1].t3()
    norm_tokens(512, 512)
    bcv.s4()
    A(0, outw.s4)
    up.s2()
    down.p1()
    B(0)
    A(1)
    C(0)
    B(1)
    A(2)
    down.s1()
    D(0)
    C(1)
    B(2)
    A(3)
    up.s3()
    E(0)
    D(1)
    C(2)
    B(3)
    down.s2()
    F(0)
    E(1)
    D(2)
    C(3)
    F(1)
    E(2)
    D(3)
    early.drain()
    up.s4()
    G(0)
    F(2)
    E(3)
    down.s3()
    G(1)
    F(3)
    G(2)
    G(3)
    down.s4()
    H(0)
    ffn[0].b()
    H(1)
    ffn[0].c()
    ffn[1].b()
    H(2)
    D2(0)
    ffn[1].c()
    ffn[2].b()
    H(3)
    D2(1)
    ffn[2].c()
    ffn[3].b()
    D2(2)
    ffn[3].c()
    D2(3)

    waits = []
    for dy, dc, dev in peers:
        source = lax.rem(h.y + 4 - dy, 4) * 2 + lax.rem(h.c + 2 - dc, 2)
        waits.append(link.same(ST.at[h.col], ST.at[source], dev))
    for wait in waits:
        wait()
    factors = mean_factor(sum(ST[k] for k in range(8)))
    for s in range(NSEQ):
        rows = pl.ds(s * LEN, LEN)
        wide = jnp.broadcast_to(factors[s : s + 1, :], (128, LEN)).T
        wide = jnp.concatenate([wide, wide], axis=1)
        closing = OWN[rows, :] * wide * consts[3:4, own_cols]
        out[rows, :] = (X[h.c, h.y, rows, :].astype(F32) + closing).astype(BF16)
    link.drain()


def body(
    tokens, mix_in_gain, bgate_weight, cgate_weight, value_weight, conv_taps, out_weight,
    mix_out_gain, ffn_in_gain, up_weight, down_weight, ffn_out_gain,
):
    gains = jnp.stack([mix_in_gain, mix_out_gain, ffn_in_gain, ffn_out_gain])
    consts = jnp.concatenate([gains, conv_taps, conv_taps[:1]]).astype(F32)
    hbm = pl.BlockSpec(memory_space=pl.ANY)
    vmem = pl.BlockSpec(memory_space=pltpu.VMEM)
    reduce_scratch = [
        pltpu.VMEM((2, 4, ROWS, W), BF16),
        pltpu.VMEM((4, ROWS, W), BF16),
        pltpu.VMEM((2, NSEQ, LEN // 2, W), BF16),
        pltpu.VMEM((2, ROWS, W), BF16),
    ]
    return pl.pallas_call(
        kernel,
        out_shape=jax.ShapeDtypeStruct((ROWS, W), BF16),
        in_specs=[hbm] * 7 + [vmem],
        out_specs=vmem,
        scratch_shapes=[
            pltpu.VMEM((2, 4, ROWS, W), BF16),
            pltpu.VMEM((2, 4, ROWS, W), BF16),
            pltpu.VMEM((ROWS, 8 * W), BF16),
            pltpu.VMEM((4, 512, 3 * W), BF16),
            pltpu.VMEM((4, W, 512), BF16),
            pltpu.VMEM((4, 512, 4 * W), BF16),
            pltpu.VMEM((4, 4 * W, 512), BF16),
            pltpu.VMEM((ROWS, 4 * W), BF16),
            *reduce_scratch,
            *reduce_scratch,
            pltpu.VMEM((ROWS, W), F32),
            pltpu.VMEM((8, 8, W), F32),
            pltpu.SemaphoreType.DMA((NSEM,)),
            pltpu.SemaphoreType.DMA((NSEM,)),
            pltpu.SemaphoreType.DMA((7,)),
        ],
        compiler_params=pltpu.CompilerParams(
            collective_id=0, has_side_effects=True, vmem_limit_bytes=64 * 1024 * 1024 - 65536
        ),
    )(tokens, bgate_weight, cgate_weight, value_weight, out_weight, up_weight, down_weight, consts)


def solution(mesh):
    torus = Mesh(mesh.devices.reshape(2, 4, 4, 4, 2), ("r", "z", "x", "y", "c"))
    fs, tp = ("z", "x"), ("y", "c")
    return jax.shard_map(
        body,
        mesh=torus,
        in_specs=(
            P(("r", "z", "x"), tp), P(), P(fs, tp), P(fs, tp), P(fs, tp), P(), P(tp, fs),
            P(), P(), P(fs, tp), P(tp, fs), P(),
        ),
        out_specs=P(("r", "z", "x"), tp),
        check_vma=False,
    )
```

time: 393 us -> 148 us (0.38)
  blocking collectives: 150 us -> 0 us
  Pallas kernels: 0 us -> 143 us
  waiting for transfers between devices: 129 us -> 0 us
  starting transfers between devices: 34.2 us -> 0 us
  matrix products: 26.1 us -> 0 us
  local copies, waits for them, and re-layouts: 26.7 us -> 3.38 us
  between operations: 13.7 us -> 0.07 us
  other arithmetic: 12.6 us -> 0.64 us
    all_to_all x3 -> x0, blocking collectives: 150 us -> none  [the longest x2 109 us: sent_and_summed(): lax.all_to_all(pieces, axis, split_axis=0, concat_axis=0, tiled=True)]
    pallas_call x0 -> x1, Pallas kernels: none -> 143 us  [body(): pl.pallas_call(kernel, out_shape=jax.ShapeDtypeStruct((ROWS, W), BF16), i...]
    all_to_all x5 -> x0, waiting for transfers between devices: 66.5 us -> none  [from_everyone(): lax.all_to_all(jnp.broadcast_to(x[None], (length, *x.shape)), axis, 0, 0,...]
    all_gather x6 -> x0, waiting for transfers between devices: 59.9 us -> none  [the longest x4 37 us: all_blocks(): pieces = lax.all_gather(pieces, axes[k])]
    all_to_all x5 -> x0, starting transfers between devices: 34 us -> none  [from_everyone(): lax.all_to_all(jnp.broadcast_to(x[None], (length, *x.shape)), axis, 0, 0,...]
    dot_general x4 -> x0, matrix products: 26.1 us -> none  [the longest x1 14.6 us: body(): jnp.dot(active, whole_of(down_weight, FS, (0, 1), 1), preferred_element_t...]
    transpose x3 -> x0, local copies, waits for them, and re-layouts: 15.9 us -> none  [the longest x2 9.5 us: all_blocks(): pieces = pieces.transpose(*back, *range(len(axes), pieces.ndim))]
    reduce_sum x8 -> x0, other arithmetic: 7.93 us -> none  [the longest x2 6.3 us: normalize(): factor = lax.rsqrt(jnp.mean(rows * rows, axis=-1, keepdims=True) + epsilon)]
  transfers between devices with their start and end apart: 11 -> 0, of which waited for: 7 -> 0; matrix products, arithmetic and copies ran while one was open for 11% -> 0% of each run, Pallas kernels for 0% -> 0%
where the time goes in v1:
time: 148 us; the launch traced here: 147 us
  Pallas kernels  143 us (97%)
  local copies, waits for them, and re-layouts  3.38 us (2%)
    pallas_call x1, Pallas kernels, body(): pl.pallas_call(kernel, out_shape=jax.ShapeDtypeStruct((ROWS, W), BF16), i...  143 us

profile of v1, /device:TPU:1, one launch (start us, length us, event | category | flops | bytes accessed | tf_op | source)
XLA Modules:
  0.0 147.5 jit_solution(15408779974131692778)
XLA Ops:
  0.0 0.0 copy-start.1
  0.0 0.0 copy-start.2
  0.0 0.7 stack.12
  0.7 0.0 copy-done.1
  0.7 0.0 copy-start
  0.8 0.0 copy-done.2
  0.8 0.0 copy-start.3
  0.8 0.7 copy-done.3
  1.5 0.0 copy-done
  1.5 0.1 concatenate.3
  1.6 0.6 convert_element_type.3.consts
  2.2 143.4 %shard_map.118 = bf16[1024,256]{1,0:T(8,128)(2,1)} custom-call(bf16[1024,256]{1,0:T(8,128)(2,1)} %tok.1, bf16[128,256]{1,0:T(8,128)(2,1)} %bw.1, bf16[128,256]{1,0:T(8,128)(2,1)} %cw.1, bf16[128,256]{1,0:T(8,128)(2,1)} %vw.1, bf16[256,128]{1,0:T(8,128)(2,1)} %ow.1, bf16[128,1024]{1,0:T(8,128)(2,1)} %uw.1, bf16[1024,128]{1,0:T(8,128)(2,1)} %dw.1, ...), custom_call_target="tpu_custom_call" | custom-call | tf_op jit(solution)/shard_map/pallas_call | solution.py:479
  145.6 1.9 %copy.14 = bf16[1024,256]{1,0:T(8,128)(2,1)} copy(bf16[1024,256]{1,0:T(8,128)(2,1)} %shard_map.118) | data formatting | bytes 1048576
  (4 shorter events, 0.0 us)
Async XLA Ops:
  0.0 0.7 copy-start.1
  0.0 0.8 copy-start.2
  0.7 0.7 copy-start
  0.8 0.7 copy-start.3

commit v2 on v1

v2 whole, which is shorter than its diff:
```python
import jax
import jax.numpy as jnp
from jax import lax
from jax.experimental import pallas as pl
from jax.experimental.pallas import tpu as pltpu
from jax.sharding import Mesh
from jax.sharding import PartitionSpec as P

EPS = 1e-6
F32 = jnp.float32
BF16 = jnp.bfloat16
LEN = 256
ROWS = 1024
W = 256
NSEQ = ROWS // LEN
NSEND, NRECV = 9, 112
TILE = 64


class Link:
    def __init__(self, send, recv):
        self.send, self.recv, self.sends, self.recvs = send, recv, 0, 0

    def sender(self):
        self.sends += 1
        return self.send.at[self.sends - 1]

    def arrivals(self, n):
        first = self.recvs
        self.recvs += n
        return [self.recv.at[first + k] for k in range(n)]


def copy_of(src, dst, sent, got, device):
    return pltpu.make_async_remote_copy(
        src_ref=src, dst_ref=dst, send_sem=sent, recv_sem=got,
        device_id=device, device_id_type=pl.DeviceIdType.MESH,
    )


class Here:
    def __init__(self):
        r, z, x, y, c = (lax.axis_index(n) for n in ("r", "z", "x", "y", "c"))
        self.z, self.x, self.y, self.c = z, x, y, c
        plus = lambda v, k, n: lax.rem(v + k, n)
        self.xp, self.xo, self.xm = (plus(x, k, 4) for k in (1, 2, 3))
        self.yp, self.yo, self.ym = (plus(y, k, 4) for k in (1, 2, 3))
        self.zp, self.zo, self.zm = (plus(z, k, 4) for k in (1, 2, 3))
        self.cn = 1 - c
        up, down = plus(r * 4 + z, 1, 8), plus(r * 4 + z, 7, 8)
        self.to_xp, self.to_xm = {"x": self.xp}, {"x": self.xm}
        self.to_yp, self.to_ym = {"y": self.yp}, {"y": self.ym}
        self.to_zp = {"r": up // 4, "z": lax.rem(up, 4)}
        self.to_zm = {"r": down // 4, "z": lax.rem(down, 4)}
        self.to_mate = {"c": self.cn}
        self.col = y * 2 + c


def at128(v, n=128):
    return pl.ds(pl.multiple_of(v * 128, 128), n)


class Group:
    def __init__(self, link, here):
        self.h, self.sent = here, link.sender()

    def go(self, src, dst, got, device):
        copy_of(src, dst, self.sent, got, device).start()

    def same(self, mine, got, device):
        self.go(mine, mine, got, device)

    def landed(self, ref, got):
        copy_of(ref, ref, self.sent, got, self.h.to_mate).wait_recv()

    def drain(self, ref):
        copy_of(ref, ref, self.sent, self.sent, self.h.to_mate).wait_send()


class Weight:
    def __init__(self, link, here, buf, by_row):
        self.h, self.buf, self.by_row = here, buf, by_row
        self.half = (buf.shape[2] if by_row else buf.shape[1]) // 2
        self.g = Group(link, here)
        self.r1, self.r2 = link.arrivals(4), link.arrivals(1)[0]
        self.rf, self.rg = link.arrivals(4), link.arrivals(1)[0]

    def unit(self, z, x, part, half=None):
        if self.by_row:
            start, n = (0, 128) if half is None else (64 * half, 64)
            rows = pl.ds(pl.multiple_of(x * 128 + start, 64), n)
            return self.buf.at[z, rows, pl.ds(part * self.half, self.half)]
        q = self.half // 2
        rows = pl.ds(part * self.half, self.half) if half is None else pl.ds(part * self.half + half * q, q)
        return self.buf.at[z, rows, at128(x)]

    def line_a(self, z, half):
        if self.by_row:
            return self.buf.at[z, pl.ds(256 * half, 256), pl.ds(0, self.half)]
        q = self.half // 2
        return self.buf.at[z, pl.ds(q * half, q), :]

    def line_b(self, x, half):
        if self.by_row:
            return self.buf.at[pl.ds(2 * half, 2), at128(x), pl.ds(self.half, self.half)]
        return self.buf.at[pl.ds(2 * half, 2), pl.ds(self.half, self.half), at128(x)]

    def p1(self):
        h, s = self.h, self.g.same
        a, b = self.unit(h.z, h.x, 0), self.unit(h.z, h.x, 1)
        for src, got, dev in zip((a, a, b, b), self.r1, (h.to_xp, h.to_xm, h.to_zp, h.to_zm)):
            s(src, got, dev)

    def s1(self):
        h, u = self.h, self.unit
        for k, (at, dev) in enumerate((
            ((h.z, h.xm, 0), h.to_xp), ((h.z, h.xp, 0), h.to_xm),
            ((h.zm, h.x, 1), h.to_zp), ((h.zp, h.x, 1), h.to_zm),
        )):
            self.g.landed(u(*at), self.r1[k])
            self.g.same(u(*at, k % 2), self.r2, dev)

    def s2(self):
        h, s, a, b = self.h, self.g.same, self.line_a, self.line_b
        quarters = (
            self.buf.at[0, pl.ds(0, 256), pl.ds(0, self.half)] if self.by_row
            else self.buf.at[0, pl.ds(0, self.half), pl.ds(0, 256)]
        )
        self.g.landed(quarters, self.r2)
        s(a(h.z, 0), self.rf[0], h.to_zp)
        s(a(h.z, 1), self.rf[1], h.to_zm)
        s(b(h.x, 0), self.rf[2], h.to_xp)
        s(b(h.x, 1), self.rf[3], h.to_xm)
        s(a(h.z, 1), self.rg, h.to_zp)
        s(a(h.z, 0), self.rg, h.to_zm)
        s(b(h.x, 1), self.rg, h.to_xp)
        s(b(h.x, 0), self.rg, h.to_xm)

    def s3(self):
        h, a, b = self.h, self.line_a, self.line_b
        for k, (ref, dev) in enumerate((
            (a(h.zm, 0), h.to_zp), (a(h.zp, 1), h.to_zm), (b(h.xm, 0), h.to_xp), (b(h.xp, 1), h.to_xm),
        )):
            self.g.landed(ref, self.rf[k])
            self.g.same(ref, self.rg, dev)

    def s4(self):
        self.g.landed(self.buf.at[pl.ds(0, 2)], self.rg)

    def drain(self):
        self.g.drain(self.buf.at[:, pl.ds(0, self.buf.shape[1] // 16 * 15), :])


class Gather:
    def __init__(self, link, group, buf, row, n):
        self.s, self.h, self.buf, self.row, self.n = group, group.h, buf, row, n
        self.f, self.g = link.arrivals(2), link.arrivals(2)
        self.far, self.mate = link.arrivals(2)

    def piece(self, c, y, half=None):
        if half is None:
            return self.buf.at[c, y, pl.ds(self.row, self.n)]
        return self.buf.at[c, y, pl.ds(self.row + half * (self.n // 2), self.n // 2)]

    def t0(self):
        h, s, p = self.h, self.s.same, self.piece
        c, y = h.c, h.y
        s(p(c, y, 0), self.f[0], h.to_yp)
        s(p(c, y, 1), self.f[1], h.to_ym)
        s(p(c, y, 1), self.g[0], h.to_yp)
        s(p(c, y, 0), self.g[1], h.to_ym)
        s(p(c, y), self.mate, h.to_mate)

    def t1(self):
        h, s, p = self.h, self.s.same, self.piece
        c, got = h.c, self.s.landed
        for k, y, dev in ((0, h.ym, h.to_yp), (1, h.yp, h.to_ym)):
            got(p(c, y, k), self.f[k])
            s(p(c, y, k), self.far, dev)
        for k, y in ((0, h.ym), (1, h.yp)):
            got(p(c, y, 1 - k), self.g[k])
            s(p(c, y), self.mate, h.to_mate)

    def t2(self):
        h, p = self.h, self.piece
        self.s.landed(p(h.c, h.yo), self.far)
        self.s.same(p(h.c, h.yo), self.mate, h.to_mate)

    def t3(self):
        self.s.landed(self.buf.at[self.h.cn, :, pl.ds(self.row, self.n)], self.mate)


class Reduce:
    def __init__(self, link, group, part, mate, r1, r2, seq):
        self.s, self.h, self.part, self.mate, self.r1, self.r2 = group, group.h, part, mate, r1, r2
        self.seq, self.row = seq, seq * LEN
        self.w0, self.w1, self.w2 = link.arrivals(1)[0], link.arrivals(2), link.arrivals(1)[0]

    def start(self):
        h, rows = self.h, pl.ds(self.row, LEN)
        self.s.go(self.part.at[h.cn, :, rows], self.mate.at[:, rows], self.w0, h.to_mate)

    def both(self, y, lo=0, n=LEN):
        rows = pl.ds(self.row + lo, n)
        return self.part[self.h.c, y, rows, :].astype(F32) + self.mate[y, rows, :].astype(F32)

    def b(self):
        h, half = self.h, LEN // 2
        self.s.landed(self.mate.at[:, pl.ds(self.row, LEN)], self.w0)
        for k, dev in ((0, h.to_yp), (1, h.to_ym)):
            rows = pl.ds(self.row + k * half, half)
            self.part[h.c, h.yo, rows, :] = self.both(h.yo, k * half, half).astype(BF16)
            self.s.go(self.part.at[h.c, h.yo, rows], self.r1.at[k, self.seq], self.w1[k], dev)

    def c(self):
        h, half = self.h, LEN // 2
        rows = pl.ds(self.row, LEN)
        for k, y, dev in ((0, h.yp, h.to_yp), (1, h.ym, h.to_ym)):
            self.s.landed(self.r1.at[k, self.seq], self.w1[k])
            add = self.r1[k, self.seq].astype(F32)
            near, far = self.both(y, k * half, half) + add, self.both(y, (1 - k) * half, half)
            self.part[h.c, y, pl.ds(self.row + k * half, half), :] = near.astype(BF16)
            self.part[h.c, y, pl.ds(self.row + (1 - k) * half, half), :] = far.astype(BF16)
            self.s.go(self.part.at[h.c, y, rows], self.r2.at[k, rows], self.w2, dev)

    def d(self):
        rows = pl.ds(self.row, LEN)
        self.s.landed(self.r2.at[:, rows], self.w2)
        return self.both(self.h.y) + self.r2[0, rows, :].astype(F32) + self.r2[1, rows, :].astype(F32)


def mean_factor(total):
    return lax.rsqrt(total * (1.0 / (8 * W)) + EPS)


def kernel(
    tok, bw, cw, vw, ow, uw, dw, g0, g1, g2, g3, taps3, out,
    consts, ga, gb, gc, gd, taps, X, M, N, WB, WO, WU, WD, ACT, PA, RDA, R1A, R2A, PB, RDB, R1B, R2B, OWN, ST,
    send, recv, local,
):
    h = Here()
    link = Link(send, recv)
    early, late, sums, last, stats = (Group(link, h) for _ in range(5))
    own_rows = at128(h.x)
    loads = [
        pltpu.make_async_copy(tok, X.at[h.c, h.y], local.at[0]),
        pltpu.make_async_copy(bw, WB.at[h.z, own_rows, pl.ds(0, W)], local.at[1]),
        pltpu.make_async_copy(cw, WB.at[h.z, own_rows, pl.ds(W, W)], local.at[2]),
        pltpu.make_async_copy(vw, WB.at[h.z, own_rows, pl.ds(2 * W, W)], local.at[3]),
        pltpu.make_async_copy(ow, WO.at[h.z, :, own_rows], local.at[4]),
        pltpu.make_async_copy(uw, WU.at[h.z, own_rows, :], local.at[5]),
        pltpu.make_async_copy(dw, WD.at[h.z, :, own_rows], local.at[6]),
    ] + [
        pltpu.make_async_copy(src, dst, local.at[7 + k])
        for k, (src, dst) in enumerate(((g0, ga), (g1, gb), (g2, gc), (g3, gd), (taps3, taps)))
    ]
    for load in loads:
        load.start()

    peers = [
        {"y": lax.rem(h.y + dy, 4), "c": lax.rem(h.c + dc, 2)}
        for dy in range(4) for dc in range(2) if dy or dc
    ]
    barrier = pltpu.get_barrier_semaphore()
    targets = [h.to_xp, h.to_xm, h.to_zp, h.to_zm] + peers
    for dev in targets:
        pl.semaphore_signal(barrier, inc=1, device_id=dev, device_id_type=pl.DeviceIdType.MESH)
    pl.semaphore_wait(barrier, len(targets))

    toks = [Gather(link, early, X, t * 512, 512) for t in range(2)]
    bcv, outw = Weight(link, h, WB, True), Weight(link, h, WO, False)
    up, down = Weight(link, h, WU, True), Weight(link, h, WD, False)
    mix = [Reduce(link, sums, PA, RDA, R1A, R2A, s) for s in range(NSEQ)]
    ffn = [Reduce(link, last, PB, RDB, R1B, R2B, s) for s in range(NSEQ)]
    mids = [Gather(link, late, M, s * LEN, LEN) for s in range(NSEQ)]

    def total(pieces):
        squares = sum(p * p for p in pieces)
        return jnp.sum(squares, axis=1, keepdims=True)

    def gain(k, j):
        return consts[k : k + 1, j * W : (j + 1) * W]

    def blocks(buf, rows):
        return [buf.at[j % 2, j // 2, rows, :] for j in range(8)]

    def scale_out(source, rows, which):
        factor = mean_factor(total([ref[...].astype(F32) for ref in blocks(source, rows)]))
        for j, ref in enumerate(blocks(source, rows)):
            N[rows, j * W : (j + 1) * W] = (ref[...].astype(F32) * factor * gain(which, j)).astype(BF16)

    def norm_tokens(first, count):
        def tile(i, carry):
            scale_out(X, pl.ds(pl.multiple_of(first + i * TILE, TILE), TILE), 0)
            return carry

        lax.fori_loop(0, count // TILE, tile, 0)

    position = lax.broadcasted_iota(jnp.int32, (LEN, W), 0)
    own_cols = pl.ds(pl.multiple_of(h.col * W, W), W)

    def mixer(s):
        rows = pl.ds(s * LEN, LEN)
        three = jnp.dot(N[rows, :], WB[...].reshape(8 * W, 3 * W), preferred_element_type=F32)
        b, c, v = (three[:, k * W : (k + 1) * W].astype(BF16).astype(F32) for k in range(3))
        inner = c * v
        before = jnp.where(position == 0, 0.0, pltpu.roll(inner, 1, 0))
        after = jnp.where(position == LEN - 1, 0.0, pltpu.roll(inner, LEN - 1, 0))
        tap = [consts[4 + k : 5 + k, own_cols] for k in range(3)]
        conv = tap[0] * before + tap[1] * inner + tap[2] * after
        return (b * conv).astype(BF16)

    def spread(left, weight, part, s):
        rows = pl.ds(s * LEN, LEN)
        for y in range(4):
            piece = jnp.dot(left, weight[y], preferred_element_type=F32).astype(BF16)
            part[0, y, rows, :] = piece[:, :W]
            part[1, y, rows, :] = piece[:, W:]

    def A(s, before_out=None):
        gated = mixer(s)
        if before_out:
            before_out()
        spread(gated, WO, PA, s)
        mix[s].start()

    def B(s):
        mix[s].b()

    def C(s):
        mix[s].c()

    def D(s):
        M[h.c, h.y, pl.ds(s * LEN, LEN), :] = mix[s].d().astype(BF16)
        mids[s].t0()

    def E(s):
        mids[s].t1()

    def F(s):
        mids[s].t2()

    def G(s):
        mids[s].t3()

        def tile(i, carry):
            rows = pl.ds(pl.multiple_of(s * LEN + i * TILE, TILE), TILE)
            mixed, kept = blocks(M, rows), blocks(X, rows)
            factor = mean_factor(total([ref[...].astype(F32) for ref in mixed]))
            for j in range(8):
                add = mixed[j][...].astype(F32) * factor * gain(1, j)
                kept[j][...] = (kept[j][...].astype(F32) + add).astype(BF16)
            scale_out(X, rows, 2)
            return carry

        lax.fori_loop(0, LEN // TILE, tile, 0)
        rows = pl.ds(s * LEN, LEN)
        lifted = jnp.dot(N[rows, :], WU[...].reshape(8 * W, 4 * W), preferred_element_type=F32)
        lifted = jnp.maximum(lifted, 0.0)
        ACT[rows, :] = (lifted * lifted).astype(BF16)

    def H(s):
        spread(ACT[pl.ds(s * LEN, LEN), :], WD, PB, s)
        ffn[s].start()

    def D2(s):
        own = ffn[s].d()
        OWN[pl.ds(s * LEN, LEN), :] = own
        energy = jnp.sum((own * own).T, axis=0, keepdims=True)
        ST[s, h.col] = jnp.broadcast_to(energy, (8, W))
        for dev in peers:
            stats.same(ST.at[s, h.col], known[s], dev)

    def finish(s):
        stats.landed(ST.at[s, pl.ds(0, 7)], known[s])
        factor = mean_factor(sum(ST[s, k] for k in range(8)))
        rows = pl.ds(s * LEN, LEN)
        wide = jnp.broadcast_to(factor[:1, :], (128, LEN)).T
        wide = jnp.concatenate([wide, wide], axis=1)
        closing = OWN[rows, :] * wide * consts[3:4, own_cols]
        out[rows, :] = (X[h.c, h.y, rows, :].astype(F32) + closing).astype(BF16)

    known = link.arrivals(NSEQ)

    loads[0].wait()
    toks[0].t0()
    toks[1].t0()
    for load in loads[1:4]:
        load.wait()
    bcv.p1()
    loads[4].wait()
    outw.p1()
    loads[5].wait()
    up.p1()
    loads[6].wait()
    for load in loads[7:]:
        load.wait()
    for k, g in enumerate((ga, gb, gc, gd)):
        consts[k : k + 1, :] = g[...].astype(F32)[None, :]
    consts[4:7, :] = taps[...].astype(F32)

    bcv.s1()
    outw.s1()
    bcv.s2()
    toks[0].t1()
    outw.s2()
    toks[1].t1()
    toks[0].t2()
    bcv.s3()
    toks[0].t3()
    norm_tokens(0, 512)
    toks[1].t2()
    outw.s3()
    up.s1()
    down.p1()
    toks[1].t3()
    norm_tokens(512, 512)
    bcv.s4()
    A(0, outw.s4)
    up.s2()
    A(1)
    B(0)
    A(2)
    B(1)
    C(0)
    down.s1()
    A(3)
    B(2)
    C(1)
    D(0)
    up.s3()
    B(3)
    C(2)
    D(1)
    down.s2()
    E(0)
    C(3)
    D(2)
    E(1)
    early.drain(X.at[:, :, pl.ds(0, 896)])
    F(0)
    D(3)
    down.s3()
    up.s4()
    G(0)
    E(2)
    F(1)
    E(3)
    F(2)
    G(1)
    F(3)
    down.s4()
    H(0)
    G(2)
    ffn[0].b()
    H(1)
    G(3)
    ffn[1].b()
    ffn[0].c()
    H(2)
    H(3)
    ffn[2].b()
    ffn[1].c()
    D2(0)
    ffn[3].b()
    ffn[2].c()
    D2(1)
    finish(0)
    ffn[3].c()
    D2(2)
    finish(1)
    D2(3)
    finish(2)
    finish(3)
    late.drain(M.at[:, :, pl.ds(0, 896)])
    sums.drain(PA.at[:, :, pl.ds(0, 896)])
    last.drain(PB.at[:, :, pl.ds(0, 896)])
    stats.drain(ST.at[:, pl.ds(0, 7)])
    for weight in (bcv, outw, up, down):
        weight.drain()


def body(
    tokens, mix_in_gain, bgate_weight, cgate_weight, value_weight, conv_taps, out_weight,
    mix_out_gain, ffn_in_gain, up_weight, down_weight, ffn_out_gain,
):
    hbm = pl.BlockSpec(memory_space=pltpu.HBM)
    vmem = pl.BlockSpec(memory_space=pltpu.VMEM)
    reduce_scratch = [
        pltpu.VMEM((2, 4, ROWS, W), BF16),
        pltpu.VMEM((4, ROWS, W), BF16),
        pltpu.VMEM((2, NSEQ, LEN // 2, W), BF16),
        pltpu.VMEM((2, ROWS, W), BF16),
    ]
    return pl.pallas_call(
        kernel,
        out_shape=jax.ShapeDtypeStruct((ROWS, W), BF16),
        in_specs=[hbm] * 12,
        out_specs=vmem,
        scratch_shapes=[
            pltpu.VMEM((8, 8 * W), F32),
            *[pltpu.VMEM((8 * W,), BF16)] * 4,
            pltpu.VMEM((3, 8 * W), BF16),
            pltpu.VMEM((2, 4, ROWS, W), BF16),
            pltpu.VMEM((2, 4, ROWS, W), BF16),
            pltpu.VMEM((ROWS, 8 * W), BF16),
            pltpu.VMEM((4, 512, 3 * W), BF16),
            pltpu.VMEM((4, W, 512), BF16),
            pltpu.VMEM((4, 512, 4 * W), BF16),
            pltpu.VMEM((4, 4 * W, 512), BF16),
            pltpu.VMEM((ROWS, 4 * W), BF16),
            *reduce_scratch,
            *reduce_scratch,
            pltpu.VMEM((ROWS, W), F32),
            pltpu.VMEM((NSEQ, 8, 8, W), F32),
            pltpu.SemaphoreType.DMA((NSEND,)),
            pltpu.SemaphoreType.DMA((NRECV,)),
            pltpu.SemaphoreType.DMA((12,)),
        ],
        compiler_params=pltpu.CompilerParams(
            collective_id=0, has_side_effects=True, vmem_limit_bytes=64 * 1024 * 1024 - 65536
        ),
    )(tokens, bgate_weight, cgate_weight, value_weight, out_weight, up_weight, down_weight,
      mix_in_gain, mix_out_gain, ffn_in_gain, ffn_out_gain, conv_taps)


def solution(mesh):
    torus = Mesh(mesh.devices.reshape(2, 4, 4, 4, 2), ("r", "z", "x", "y", "c"))
    fs, tp = ("z", "x"), ("y", "c")
    return jax.shard_map(
        body,
        mesh=torus,
        in_specs=(
            P(("r", "z", "x"), tp), P(), P(fs, tp), P(fs, tp), P(fs, tp), P(), P(tp, fs),
            P(), P(), P(fs, tp), P(tp, fs), P(),
        ),
        out_specs=P(("r", "z", "x"), tp),
        check_vma=False,
    )
```

time: 148 us -> 115 us (0.78)
  Pallas kernels: 143 us -> 113 us
  local copies, waits for them, and re-layouts: 3.38 us -> 1.87 us
    pallas_call x1, Pallas kernels: 143 us -> 113 us  [body(): pl.pallas_call(kernel, out_shape=jax.ShapeDtypeStruct((ROWS, W), BF16), i...]
where the time goes in v2:
time: 115 us
  Pallas kernels  113 us (98%)
  local copies, waits for them, and re-layouts  1.87 us (2%)
    pallas_call x1, Pallas kernels, body(): pl.pallas_call(kernel, out_shape=jax.ShapeDtypeStruct((ROWS, W), BF16), i...  113 us

profile of v2, /device:TPU:1, one launch (start us, length us, event | category | flops | bytes accessed | tf_op | source)
XLA Modules:
  0.0 115.4 jit_solution(13182664025833769928)
XLA Ops:
  0.0 113.5 %shard_map.118 = bf16[1024,256]{1,0:T(8,128)(2,1)} custom-call(bf16[1024,256]{1,0:T(8,128)(2,1)} %tok.1, bf16[128,256]{1,0:T(8,128)(2,1)} %bw.1, bf16[128,256]{1,0:T(8,128)(2,1)} %cw.1, bf16[128,256]{1,0:T(8,128)(2,1)} %vw.1, bf16[256,128]{1,0:T(8,128)(2,1)} %ow.1, bf16[128,1024]{1,0:T(8,128)(2,1)} %uw.1, bf16[1024,128]{1,0:T(8,128)(2,1)} %dw.1, ...), custom_call_target="tpu_custom_call" | custom-call | tf_op jit(solution)/shard_map/pallas_call | solution.py:495
  113.5 1.9 %copy.14 = bf16[1024,256]{1,0:T(8,128)(2,1)} copy(bf16[1024,256]{1,0:T(8,128)(2,1)} %shard_map.118) | data formatting | bytes 1048576

commit v3 on v2

--- a/solution.py
+++ b/solution.py
@@ -13,7 +13,7 @@
 ROWS = 1024
 W = 256
 NSEQ = ROWS // LEN
-NSEND, NRECV = 9, 112
+NSEND, NRECV = 9, 120
 TILE = 64
 
 
@@ -94,55 +94,58 @@
         rows = pl.ds(part * self.half, self.half) if half is None else pl.ds(part * self.half + half * q, q)
         return self.buf.at[z, rows, at128(x)]
 
-    def line_a(self, z, half):
-        if self.by_row:
-            return self.buf.at[z, pl.ds(256 * half, 256), pl.ds(0, self.half)]
-        q = self.half // 2
-        return self.buf.at[z, pl.ds(q * half, q), :]
-
-    def line_b(self, x, half):
-        if self.by_row:
-            return self.buf.at[pl.ds(2 * half, 2), at128(x), pl.ds(self.half, self.half)]
-        return self.buf.at[pl.ds(2 * half, 2), pl.ds(self.half, self.half), at128(x)]
-
-    def p1(self):
-        h, s = self.h, self.g.same
-        a, b = self.unit(h.z, h.x, 0), self.unit(h.z, h.x, 1)
-        for src, got, dev in zip((a, a, b, b), self.r1, (h.to_xp, h.to_xm, h.to_zp, h.to_zm)):
-            s(src, got, dev)
-
-    def s1(self):
-        h, u = self.h, self.unit
-        for k, (at, dev) in enumerate((
+    def neighbours(self):
+        h = self.h
+        return (
             ((h.z, h.xm, 0), h.to_xp), ((h.z, h.xp, 0), h.to_xm),
             ((h.zm, h.x, 1), h.to_zp), ((h.zp, h.x, 1), h.to_zm),
-        )):
-            self.g.landed(u(*at), self.r1[k])
-            self.g.same(u(*at, k % 2), self.r2, dev)
+        )
+
+    def p1(self, early):
+        h = self.h
+        for k, (_, dev) in enumerate(self.neighbours()):
+            half = k % 2 if early else 1 - k % 2
+            self.g.same(self.unit(h.z, h.x, k // 2, half), self.r1[k] if early else self.r2, dev)
+
+    def s1(self):
+        for k, (at, dev) in enumerate(self.neighbours()):
+            ref = self.unit(*at, k % 2)
+            self.g.landed(ref, self.r1[k])
+            self.g.same(ref, self.r2, dev)
+
+    def second(self):
+        h, u = self.h, self.unit
+        a = [lambda z, x=x: u(z, x, 0) for x in (h.x, h.xp, h.xo, h.xm)]
+        b = [lambda x, z=z: u(z, x, 1) for z in (h.z, h.zp, h.zo, h.zm)]
+        return (
+            (a, h.z, h.zm, (0, 1), (2, 3), h.to_zp), (a, h.z, h.zp, (2, 3), (0, 1), h.to_zm),
+            (b, h.x, h.xm, (0, 1), (2, 3), h.to_xp), (b, h.x, h.xp, (2, 3), (0, 1), h.to_xm),
+        )
+
+    def own2(self):
+        for k, (line, here, _, passed, _, dev) in enumerate(self.second()):
+            self.g.same(line[0](here), self.rf[k] if 0 in passed else self.rg, dev)
 
     def s2(self):
-        h, s, a, b = self.h, self.g.same, self.line_a, self.line_b
-        quarters = (
+        if self.by_row:
+            self.g.landed(self.buf.at[0, :, pl.ds(0, self.half)], self.r2)
+        else:
+            self.g.landed(self.buf.at[0, pl.ds(0, self.half), :], self.r2)
+        for first in (True, False):
+            for k, (line, here, _, passed, kept, dev) in enumerate(self.second()):
+                for n in passed if first else kept:
+                    if n:
+                        self.g.same(line[n](here), self.rf[k] if first else self.rg, dev)
+
+    def s3(self):
+        two = (
             self.buf.at[0, pl.ds(0, 256), pl.ds(0, self.half)] if self.by_row
             else self.buf.at[0, pl.ds(0, self.half), pl.ds(0, 256)]
         )
-        self.g.landed(quarters, self.r2)
-        s(a(h.z, 0), self.rf[0], h.to_zp)
-        s(a(h.z, 1), self.rf[1], h.to_zm)
-        s(b(h.x, 0), self.rf[2], h.to_xp)
-        s(b(h.x, 1), self.rf[3], h.to_xm)
-        s(a(h.z, 1), self.rg, h.to_zp)
-        s(a(h.z, 0), self.rg, h.to_zm)
-        s(b(h.x, 1), self.rg, h.to_xp)
-        s(b(h.x, 0), self.rg, h.to_xm)
-
-    def s3(self):
-        h, a, b = self.h, self.line_a, self.line_b
-        for k, (ref, dev) in enumerate((
-            (a(h.zm, 0), h.to_zp), (a(h.zp, 1), h.to_zm), (b(h.xm, 0), h.to_xp), (b(h.xp, 1), h.to_xm),
-        )):
-            self.g.landed(ref, self.rf[k])
-            self.g.same(ref, self.rg, dev)
+        for k, (line, _, source, passed, _, dev) in enumerate(self.second()):
+            self.g.landed(two, self.rf[k])
+            for n in passed:
+                self.g.same(line[n](source), self.rg, dev)
 
     def s4(self):
         self.g.landed(self.buf.at[pl.ds(0, 2)], self.rg)
@@ -177,6 +180,10 @@
         for k, y, dev in ((0, h.ym, h.to_yp), (1, h.yp, h.to_ym)):
             got(p(c, y, k), self.f[k])
             s(p(c, y, k), self.far, dev)
+
+    def t1b(self):
+        h, s, p = self.h, self.s.same, self.piece
+        c, got = h.c, self.s.landed
         for k, y in ((0, h.ym), (1, h.yp)):
             got(p(c, y, 1 - k), self.g[k])
             s(p(c, y), self.mate, h.to_mate)
@@ -194,11 +201,11 @@
     def __init__(self, link, group, part, mate, r1, r2, seq):
         self.s, self.h, self.part, self.mate, self.r1, self.r2 = group, group.h, part, mate, r1, r2
         self.seq, self.row = seq, seq * LEN
-        self.w0, self.w1, self.w2 = link.arrivals(1)[0], link.arrivals(2), link.arrivals(1)[0]
-
-    def start(self):
+        self.w0, self.w1, self.w2 = link.arrivals(2), link.arrivals(2), link.arrivals(1)[0]
+
+    def start(self, y, k):
         h, rows = self.h, pl.ds(self.row, LEN)
-        self.s.go(self.part.at[h.cn, :, rows], self.mate.at[:, rows], self.w0, h.to_mate)
+        self.s.go(self.part.at[h.cn, y, rows], self.mate.at[y, rows], self.w0[k], h.to_mate)
 
     def both(self, y, lo=0, n=LEN):
         rows = pl.ds(self.row + lo, n)
@@ -206,7 +213,7 @@
 
     def b(self):
         h, half = self.h, LEN // 2
-        self.s.landed(self.mate.at[:, pl.ds(self.row, LEN)], self.w0)
+        self.s.landed(self.mate.at[h.yo, pl.ds(self.row, LEN)], self.w0[0])
         for k, dev in ((0, h.to_yp), (1, h.to_ym)):
             rows = pl.ds(self.row + k * half, half)
             self.part[h.c, h.yo, rows, :] = self.both(h.yo, k * half, half).astype(BF16)
@@ -215,6 +222,7 @@
     def c(self):
         h, half = self.h, LEN // 2
         rows = pl.ds(self.row, LEN)
+        self.s.landed(self.mate.at[pl.ds(0, 3), rows], self.w0[1])
         for k, y, dev in ((0, h.yp, h.to_yp), (1, h.ym, h.to_ym)):
             self.s.landed(self.r1.at[k, self.seq], self.w1[k])
             add = self.r1[k, self.seq].astype(F32)
@@ -235,7 +243,7 @@
 
 def kernel(
     tok, bw, cw, vw, ow, uw, dw, g0, g1, g2, g3, taps3, out,
-    consts, ga, gb, gc, gd, taps, X, M, N, WB, WO, WU, WD, ACT, PA, RDA, R1A, R2A, PB, RDB, R1B, R2B, OWN, ST,
+    consts, ga, gb, gc, gd, taps, X, M, N, WB, WO, WU, WD, ACT, PA, RDA, R1A, R2A, PB, RDB, R1B, R2B, OWN, ST, OUTV,
     send, recv, local,
 ):
     h = Here()
@@ -310,19 +318,24 @@
         conv = tap[0] * before + tap[1] * inner + tap[2] * after
         return (b * conv).astype(BF16)
 
-    def spread(left, weight, part, s):
-        rows = pl.ds(s * LEN, LEN)
-        for y in range(4):
+    def spread(left, weight, part, reduce, eager):
+        rows = pl.ds(reduce.row, LEN)
+        order = (h.yo, h.yp, h.ym, h.y)
+        for y in order if eager else range(4):
             piece = jnp.dot(left, weight[y], preferred_element_type=F32).astype(BF16)
             part[0, y, rows, :] = piece[:, :W]
             part[1, y, rows, :] = piece[:, W:]
+            if eager:
+                reduce.start(y, 0 if y is h.yo else 1)
+        if not eager:
+            for y in order:
+                reduce.start(y, 0 if y is h.yo else 1)
 
     def A(s, before_out=None):
         gated = mixer(s)
         if before_out:
             before_out()
-        spread(gated, WO, PA, s)
-        mix[s].start()
+        spread(gated, WO, PA, mix[s], s == 0)
 
     def B(s):
         mix[s].b()
@@ -334,13 +347,16 @@
         M[h.c, h.y, pl.ds(s * LEN, LEN), :] = mix[s].d().astype(BF16)
         mids[s].t0()
 
-    def E(s):
+    def Ea(s):
         mids[s].t1()
+
+    def Eb(s):
+        mids[s].t1b()
 
     def F(s):
         mids[s].t2()
 
-    def G(s):
+    def Ga(s):
         mids[s].t3()
 
         def tile(i, carry):
@@ -354,20 +370,21 @@
             return carry
 
         lax.fori_loop(0, LEN // TILE, tile, 0)
+
+    def Gb(s):
         rows = pl.ds(s * LEN, LEN)
         lifted = jnp.dot(N[rows, :], WU[...].reshape(8 * W, 4 * W), preferred_element_type=F32)
         lifted = jnp.maximum(lifted, 0.0)
         ACT[rows, :] = (lifted * lifted).astype(BF16)
 
     def H(s):
-        spread(ACT[pl.ds(s * LEN, LEN), :], WD, PB, s)
-        ffn[s].start()
+        spread(ACT[pl.ds(s * LEN, LEN), :], WD, PB, ffn[s], s == 0)
 
     def D2(s):
         own = ffn[s].d()
         OWN[pl.ds(s * LEN, LEN), :] = own
         energy = jnp.sum((own * own).T, axis=0, keepdims=True)
-        ST[s, h.col] = jnp.broadcast_to(energy, (8, W))
+        ST[s, h.col] = energy
         for dev in peers:
             stats.same(ST.at[s, h.col], known[s], dev)
 
@@ -375,101 +392,119 @@
         stats.landed(ST.at[s, pl.ds(0, 7)], known[s])
         factor = mean_factor(sum(ST[s, k] for k in range(8)))
         rows = pl.ds(s * LEN, LEN)
-        wide = jnp.broadcast_to(factor[:1, :], (128, LEN)).T
+        wide = jnp.broadcast_to(factor, (128, LEN)).T
         wide = jnp.concatenate([wide, wide], axis=1)
         closing = OWN[rows, :] * wide * consts[3:4, own_cols]
-        out[rows, :] = (X[h.c, h.y, rows, :].astype(F32) + closing).astype(BF16)
-
-    known = link.arrivals(NSEQ)
+        OUTV[rows, :] = (X[h.c, h.y, rows, :].astype(F32) + closing).astype(BF16)
+        stored.append(pltpu.make_async_copy(OUTV.at[rows], out.at[rows], local.at[12 + s]))
+        stored[-1].start()
+
+    known, stored = link.arrivals(NSEQ), []
 
     loads[0].wait()
     toks[0].t0()
     toks[1].t0()
     for load in loads[1:4]:
         load.wait()
-    bcv.p1()
+    bcv.p1(True)
+    bcv.p1(False)
     loads[4].wait()
-    outw.p1()
-    loads[5].wait()
-    up.p1()
-    loads[6].wait()
-    for load in loads[7:]:
+    outw.p1(True)
+    outw.p1(False)
+    for load in loads[5:]:
         load.wait()
     for k, g in enumerate((ga, gb, gc, gd)):
         consts[k : k + 1, :] = g[...].astype(F32)[None, :]
     consts[4:7, :] = taps[...].astype(F32)
 
     bcv.s1()
+    bcv.own2()
+    up.p1(True)
     outw.s1()
+    outw.own2()
     bcv.s2()
+    outw.s2()
     toks[0].t1()
-    outw.s2()
+    toks[0].t1b()
+    bcv.s3()
     toks[1].t1()
+    toks[1].t1b()
     toks[0].t2()
-    bcv.s3()
     toks[0].t3()
     norm_tokens(0, 512)
+    outw.s3()
     toks[1].t2()
-    outw.s3()
+    up.p1(False)
     up.s1()
-    down.p1()
     toks[1].t3()
     norm_tokens(512, 512)
     bcv.s4()
+    up.own2()
+    down.p1(True)
+    down.p1(False)
     A(0, outw.s4)
+    B(0)
+    A(1)
     up.s2()
-    A(1)
-    B(0)
-    A(2)
     B(1)
     C(0)
-    down.s1()
-    A(3)
+    A(2)
     B(2)
     C(1)
+    down.s1()
+    down.own2()
+    A(3)
+    B(3)
     D(0)
     up.s3()
-    B(3)
     C(2)
+    Ea(0)
     D(1)
+    C(3)
+    Eb(0)
     down.s2()
-    E(0)
-    C(3)
+    F(0)
+    Ea(1)
     D(2)
-    E(1)
+    Eb(1)
     early.drain(X.at[:, :, pl.ds(0, 896)])
-    F(0)
+    up.s4()
+    Ga(0)
+    Gb(0)
+    F(1)
+    down.s3()
     D(3)
-    down.s3()
-    up.s4()
-    G(0)
-    E(2)
-    F(1)
-    E(3)
+    Ea(2)
+    Eb(2)
+    Ga(1)
+    Ea(3)
+    Gb(1)
+    Eb(3)
     F(2)
-    G(1)
     F(3)
+    Ga(2)
+    Gb(2)
     down.s4()
     H(0)
-    G(2)
     ffn[0].b()
     H(1)
-    G(3)
+    H(2)
     ffn[1].b()
     ffn[0].c()
-    H(2)
+    ffn[2].b()
+    Ga(3)
+    Gb(3)
+    ffn[1].c()
     H(3)
-    ffn[2].b()
-    ffn[1].c()
+    ffn[3].b()
     D2(0)
-    ffn[3].b()
     ffn[2].c()
+    ffn[3].c()
     D2(1)
+    D2(2)
     finish(0)
-    ffn[3].c()
-    D2(2)
+    D2(3)
     finish(1)
-    D2(3)
     finish(2)
     finish(3)
     late.drain(M.at[:, :, pl.ds(0, 896)])
@@ -478,6 +513,8 @@
     stats.drain(ST.at[:, pl.ds(0, 7)])
     for weight in (bcv, outw, up, down):
         weight.drain()
+    for copy in stored:
+        copy.wait()
 
 
 def body(
@@ -485,7 +522,6 @@
     mix_out_gain, ffn_in_gain, up_weight, down_weight, ffn_out_gain,
 ):
     hbm = pl.BlockSpec(memory_space=pltpu.HBM)
-    vmem = pl.BlockSpec(memory_space=pltpu.VMEM)
     reduce_scratch = [
         pltpu.VMEM((2, 4, ROWS, W), BF16),
         pltpu.VMEM((4, ROWS, W), BF16),
@@ -496,7 +532,7 @@
         kernel,
         out_shape=jax.ShapeDtypeStruct((ROWS, W), BF16),
         in_specs=[hbm] * 12,
-        out_specs=vmem,
+        out_specs=hbm,
         scratch_shapes=[
             pltpu.VMEM((8, 8 * W), F32),
             *[pltpu.VMEM((8 * W,), BF16)] * 4,
@@ -512,10 +548,11 @@
             *reduce_scratch,
             *reduce_scratch,
             pltpu.VMEM((ROWS, W), F32),
-            pltpu.VMEM((NSEQ, 8, 8, W), F32),
+            pltpu.VMEM((NSEQ, 8, 1, W), F32),
+            pltpu.VMEM((ROWS, W), BF16),
             pltpu.SemaphoreType.DMA((NSEND,)),
             pltpu.SemaphoreType.DMA((NRECV,)),
-            pltpu.SemaphoreType.DMA((12,)),
+            pltpu.SemaphoreType.DMA((12 + NSEQ,)),
         ],
         compiler_params=pltpu.CompilerParams(
             collective_id=0, has_side_effects=True, vmem_limit_bytes=64 * 1024 * 1024 - 65536

time: 115 us -> 109 us (0.948)
  Pallas kernels: 113 us -> 107 us
    pallas_call x1, Pallas kernels: 113 us -> 107 us  [body(): pl.pallas_call(kernel, out_shape=jax.ShapeDtypeStruct((ROWS, W), BF16), i...]
where the time goes in v3:
time: 109 us
  Pallas kernels  107 us (98%)
  local copies, waits for them, and re-layouts  1.87 us (2%)
    pallas_call x1, Pallas kernels, body(): pl.pallas_call(kernel, out_shape=jax.ShapeDtypeStruct((ROWS, W), BF16), i...  107 us

profile of v3, /device:TPU:1, one launch (start us, length us, event | category | flops | bytes accessed | tf_op | source)
XLA Modules:
  0.0 109.0 jit_solution(1003011002988305299)
XLA Ops:
  0.0 107.2 %shard_map.118 = bf16[1024,256]{1,0:T(8,128)(2,1)} custom-call(bf16[1024,256]{1,0:T(8,128)(2,1)} %tok.1, bf16[128,256]{1,0:T(8,128)(2,1)} %bw.1, bf16[128,256]{1,0:T(8,128)(2,1)} %cw.1, bf16[128,256]{1,0:T(8,128)(2,1)} %vw.1, bf16[256,128]{1,0:T(8,128)(2,1)} %ow.1, bf16[128,1024]{1,0:T(8,128)(2,1)} %uw.1, bf16[1024,128]{1,0:T(8,128)(2,1)} %dw.1, ...), custom_call_target="tpu_custom_call" | custom-call | tf_op jit(solution)/shard_map/pallas_call | solution.py:531
  107.2 1.9 %copy.14 = bf16[1024,256]{1,0:T(8,128)(2,1)} copy(bf16[1024,256]{1,0:T(8,128)(2,1)} %shard_map.118) | data formatting | bytes 1048576

commit v4 on v3

--- a/solution.py
+++ b/solution.py
@@ -318,24 +318,27 @@
         conv = tap[0] * before + tap[1] * inner + tap[2] * after
         return (b * conv).astype(BF16)
 
-    def spread(left, weight, part, reduce, eager):
+    def spread(left, weight, part, reduce):
         rows = pl.ds(reduce.row, LEN)
-        order = (h.yo, h.yp, h.ym, h.y)
-        for y in order if eager else range(4):
+
+        def block(y):
             piece = jnp.dot(left, weight[y], preferred_element_type=F32).astype(BF16)
             part[0, y, rows, :] = piece[:, :W]
             part[1, y, rows, :] = piece[:, W:]
-            if eager:
-                reduce.start(y, 0 if y is h.yo else 1)
-        if not eager:
-            for y in order:
-                reduce.start(y, 0 if y is h.yo else 1)
+
+        block(h.yo)
+        reduce.start(h.yo, 0)
+        others = (h.yp, h.ym, h.y)
+        for y in others:
+            block(y)
+        for y in others:
+            reduce.start(y, 1)
 
     def A(s, before_out=None):
         gated = mixer(s)
         if before_out:
             before_out()
-        spread(gated, WO, PA, mix[s], s == 0)
+        spread(gated, WO, PA, mix[s])
 
     def B(s):
         mix[s].b()
@@ -378,7 +381,7 @@
         ACT[rows, :] = (lifted * lifted).astype(BF16)
 
     def H(s):
-        spread(ACT[pl.ds(s * LEN, LEN), :], WD, PB, ffn[s], s == 0)
+        spread(ACT[pl.ds(s * LEN, LEN), :], WD, PB, ffn[s])
 
     def D2(s):
         own = ffn[s].d()
@@ -411,6 +414,7 @@
     loads[4].wait()
     outw.p1(True)
     outw.p1(False)
+    bcv.own2()
     for load in loads[5:]:
         load.wait()
     for k, g in enumerate((ga, gb, gc, gd)):
@@ -418,10 +422,9 @@
     consts[4:7, :] = taps[...].astype(F32)
 
     bcv.s1()
-    bcv.own2()
-    up.p1(True)
     outw.s1()
     outw.own2()
+    up.p1(True)
     bcv.s2()
     outw.s2()
     toks[0].t1()
@@ -434,48 +437,48 @@
     norm_tokens(0, 512)
     outw.s3()
     toks[1].t2()
-    up.p1(False)
-    up.s1()
     toks[1].t3()
     norm_tokens(512, 512)
     bcv.s4()
+    up.p1(False)
     up.own2()
+    A(0, outw.s4)
+    B(0)
     down.p1(True)
     down.p1(False)
-    A(0, outw.s4)
-    B(0)
     A(1)
-    up.s2()
+    up.s1()
     B(1)
     C(0)
+    down.own2()
     A(2)
     B(2)
     C(1)
-    down.s1()
-    down.own2()
+    up.s2()
     A(3)
     B(3)
     D(0)
+    C(2)
+    down.s1()
+    Ea(0)
     up.s3()
-    C(2)
-    Ea(0)
     D(1)
     C(3)
     Eb(0)
+    F(0)
     down.s2()
-    F(0)
     Ea(1)
     D(2)
     Eb(1)
     early.drain(X.at[:, :, pl.ds(0, 896)])
-    up.s4()
     Ga(0)
-    Gb(0)
     F(1)
-    down.s3()
     D(3)
     Ea(2)
+    up.s4()
+    Gb(0)
     Eb(2)
+    down.s3()
     Ga(1)
     Ea(3)
     Gb(1)
@@ -488,17 +491,17 @@
     H(0)
     ffn[0].b()
     H(1)
+    ffn[1].b()
     H(2)
-    ffn[1].b()
+    ffn[2].b()
     ffn[0].c()
-    ffn[2].b()
     Ga(3)
     Gb(3)
     ffn[1].c()
     H(3)
     ffn[3].b()
+    ffn[2].c()
     D2(0)
-    ffn[2].c()
     ffn[3].c()
     D2(1)
     D2(2)

time: 109 us -> 106 us (0.972)
  Pallas kernels: 107 us -> 104 us
    pallas_call x1, Pallas kernels: 107 us -> 104 us  [body(): pl.pallas_call(kernel, out_shape=jax.ShapeDtypeStruct((ROWS, W), BF16), i...]
where the time goes in v4:
time: 106 us
  Pallas kernels  104 us (98%)
  local copies, waits for them, and re-layouts  1.87 us (2%)
    pallas_call x1, Pallas kernels, body(): pl.pallas_call(kernel, out_shape=jax.ShapeDtypeStruct((ROWS, W), BF16), i...  104 us

profile of v4, /device:TPU:1, one launch (start us, length us, event | category | flops | bytes accessed | tf_op | source)
XLA Modules:
  0.0 105.7 jit_solution(2125408800748831301)
XLA Ops:
  0.0 103.8 %shard_map.118 = bf16[1024,256]{1,0:T(8,128)(2,1)} custom-call(bf16[1024,256]{1,0:T(8,128)(2,1)} %tok.1, bf16[128,256]{1,0:T(8,128)(2,1)} %bw.1, bf16[128,256]{1,0:T(8,128)(2,1)} %cw.1, bf16[128,256]{1,0:T(8,128)(2,1)} %vw.1, bf16[256,128]{1,0:T(8,128)(2,1)} %ow.1, bf16[128,1024]{1,0:T(8,128)(2,1)} %uw.1, bf16[1024,128]{1,0:T(8,128)(2,1)} %dw.1, ...), custom_call_target="tpu_custom_call" | custom-call | tf_op jit(solution)/shard_map/pallas_call | solution.py:534
  103.8 1.9 %copy.14 = bf16[1024,256]{1,0:T(8,128)(2,1)} copy(bf16[1024,256]{1,0:T(8,128)(2,1)} %shard_map.118) | data formatting | bytes 1048576

commit v5 on v4

--- a/solution.py
+++ b/solution.py
@@ -440,6 +440,7 @@
     toks[1].t3()
     norm_tokens(512, 512)
     bcv.s4()
+    up.s1()
     up.p1(False)
     up.own2()
     A(0, outw.s4)
@@ -447,26 +448,25 @@
     down.p1(True)
     down.p1(False)
     A(1)
-    up.s1()
+    up.s2()
     B(1)
     C(0)
-    down.own2()
     A(2)
     B(2)
     C(1)
-    up.s2()
+    down.s1()
+    down.own2()
     A(3)
     B(3)
     D(0)
     C(2)
-    down.s1()
+    up.s3()
     Ea(0)
-    up.s3()
     D(1)
     C(3)
+    down.s2()
     Eb(0)
     F(0)
-    down.s2()
     Ea(1)
     D(2)
     Eb(1)
@@ -474,11 +474,11 @@
     Ga(0)
     F(1)
     D(3)
+    down.s3()
     Ea(2)
     up.s4()
     Gb(0)
     Eb(2)
-    down.s3()
     Ga(1)
     Ea(3)
     Gb(1)

time: 106 us -> 106 us (level)
  no operation moved by 1% of the time
where the time goes in v5:
time: 106 us
  Pallas kernels  104 us (98%)
  local copies, waits for them, and re-layouts  1.87 us (2%)
    pallas_call x1, Pallas kernels, body(): pl.pallas_call(kernel, out_shape=jax.ShapeDtypeStruct((ROWS, W), BF16), i...  104 us

profile of v5, /device:TPU:1, one launch (start us, length us, event | category | flops | bytes accessed | tf_op | source)
XLA Modules:
  0.0 106.3 jit_solution(5719089765225583087)
XLA Ops:
  0.0 104.4 %shard_map.118 = bf16[1024,256]{1,0:T(8,128)(2,1)} custom-call(bf16[1024,256]{1,0:T(8,128)(2,1)} %tok.1, bf16[128,256]{1,0:T(8,128)(2,1)} %bw.1, bf16[128,256]{1,0:T(8,128)(2,1)} %cw.1, bf16[128,256]{1,0:T(8,128)(2,1)} %vw.1, bf16[256,128]{1,0:T(8,128)(2,1)} %ow.1, bf16[128,1024]{1,0:T(8,128)(2,1)} %uw.1, bf16[1024,128]{1,0:T(8,128)(2,1)} %dw.1, ...), custom_call_target="tpu_custom_call" | custom-call | tf_op jit(solution)/shard_map/pallas_call | solution.py:534
  104.4 1.9 %copy.14 = bf16[1024,256]{1,0:T(8,128)(2,1)} copy(bf16[1024,256]{1,0:T(8,128)(2,1)} %shard_map.118) | data formatting | bytes 1048576

commit v6 on v4

--- a/solution.py
+++ b/solution.py
@@ -414,7 +414,6 @@
     loads[4].wait()
     outw.p1(True)
     outw.p1(False)
-    bcv.own2()
     for load in loads[5:]:
         load.wait()
     for k, g in enumerate((ga, gb, gc, gd)):
@@ -422,9 +421,9 @@
     consts[4:7, :] = taps[...].astype(F32)
 
     bcv.s1()
+    bcv.own2()
     outw.s1()
     outw.own2()
-    up.p1(True)
     bcv.s2()
     outw.s2()
     toks[0].t1()
@@ -440,6 +439,7 @@
     toks[1].t3()
     norm_tokens(512, 512)
     bcv.s4()
+    up.p1(True)
     up.p1(False)
     up.own2()
     A(0, outw.s4)
@@ -454,9 +454,9 @@
     A(2)
     B(2)
     C(1)
-    up.s2()
     A(3)
     B(3)
+    up.s2()
     D(0)
     C(2)
     down.s1()
@@ -478,15 +478,17 @@
     up.s4()
     Gb(0)
     Eb(2)
-    down.s3()
     Ga(1)
     Ea(3)
+    down.s3()
     Gb(1)
     Eb(3)
     F(2)
     F(3)
     Ga(2)
     Gb(2)
+    Ga(3)
+    Gb(3)
     down.s4()
     H(0)
     ffn[0].b()
@@ -495,11 +497,9 @@
     H(2)
     ffn[2].b()
     ffn[0].c()
-    Ga(3)
-    Gb(3)
-    ffn[1].c()
     H(3)
     ffn[3].b()
+    ffn[1].c()
     ffn[2].c()
     D2(0)
     ffn[3].c()

time: 106 us -> 107 us (level)
    pallas_call x1, Pallas kernels: 104 us -> 105 us  [body(): pl.pallas_call(kernel, out_shape=jax.ShapeDtypeStruct((ROWS, W), BF16), i...]
where the time goes in v6:
time: 107 us
  Pallas kernels  105 us (98%)
  local copies, waits for them, and re-layouts  1.87 us (2%)
    pallas_call x1, Pallas kernels, body(): pl.pallas_call(kernel, out_shape=jax.ShapeDtypeStruct((ROWS, W), BF16), i...  105 us

profile of v6, /device:TPU:1, one launch (start us, length us, event | category | flops | bytes accessed | tf_op | source)
XLA Modules:
  0.0 107.3 jit_solution(2372742531699723177)
XLA Ops:
  0.0 105.4 %shard_map.118 = bf16[1024,256]{1,0:T(8,128)(2,1)} custom-call(bf16[1024,256]{1,0:T(8,128)(2,1)} %tok.1, bf16[128,256]{1,0:T(8,128)(2,1)} %bw.1, bf16[128,256]{1,0:T(8,128)(2,1)} %cw.1, bf16[128,256]{1,0:T(8,128)(2,1)} %vw.1, bf16[256,128]{1,0:T(8,128)(2,1)} %ow.1, bf16[128,1024]{1,0:T(8,128)(2,1)} %uw.1, bf16[1024,128]{1,0:T(8,128)(2,1)} %dw.1, ...), custom_call_target="tpu_custom_call" | custom-call | tf_op jit(solution)/shard_map/pallas_call | solution.py:534
  105.4 1.9 %copy.14 = bf16[1024,256]{1,0:T(8,128)(2,1)} copy(bf16[1024,256]{1,0:T(8,128)(2,1)} %shard_map.118) | data formatting | bytes 1048576
